TPU v7x, 128 devices: a whole 4x4x4 slice. The times are simulated.
128 devices in a mesh: sp: 16 (over z, x), tp: 8 (over y, core).
Axes of the slice: x: 4, y: 4, z: 4, core: 2. Of those that a mesh axis runs over, the one named last changes fastest.
Arguments:
- residual: bfloat16 [12288, 4096], P('sp', 'tp'), may hold values from -40 to 40
- values: bfloat16 [12288, 2048], P('sp', 'tp'), may hold values from -6 to 6
- forget_onward: bfloat16 [12288, 2048], P('sp', 'tp'), may hold values from -5.5 to 5.5
- forget_reverse: bfloat16 [12288, 2048], P('sp', 'tp'), may hold values from -5.5 to 5.5
- surge_log_decay: float32 [12288, 16], P('sp', 'tp'), may hold values from -2.1 to 0
- gate_limit_complement: float32 [2, 2048], P(None, 'tp'), may hold values from 2.4414062e-05 to 0.1
- readout_query: bfloat16 [12288, 2048], P('sp', 'tp'), may hold values from -6 to 6
- output_gate: bfloat16 [12288, 2048], P('sp', 'tp'), may hold values from -6 to 6
- head_norm_gain: float32 [128], replicated, may hold values from 0.1 to 1.9
- output_weight: bfloat16 [2048, 4096], P('tp'), may hold values from -0.125 to 0.125
- mixer_norm_gain: float32 [4096], replicated, may hold values from 0.1 to 1.9
- up_weight: bfloat16 [4096, 8192], P('sp', 'tp'), may hold values from -0.09375 to 0.09375
- down_weight: bfloat16 [4096, 8192], P('sp', 'tp'), may hold values from -0.0625 to 0.0625
Outputs:
- output: bfloat16 [12288, 4096], P('sp', 'tp')
All inputs are finite; a program needn't handle non-finite values.
Results may differ from a plain program's by a relative error of at most 0.015.
Values may be sent and summed in bfloat16 or wider, within the bound.
A program may use at most 192 MiB of HBM per device.

v0:
```python
import jax
import jax.numpy as jnp
from jax import lax
from jax.sharding import PartitionSpec as P

D = 4096
HEAD_DIM = 128
BLOCK = 64


epsilon = 1e-06
top_precision = lax.Precision.HIGHEST


def in_order(tiles, dim):
    shape = list(tiles.shape[1:])
    shape[dim] *= tiles.shape[0]
    return jnp.moveaxis(tiles, 0, dim).reshape(shape)


def gather_packed(arrays, axis, dims):
    line = jnp.concatenate([a.reshape(-1) for a in arrays])
    lines, at, gathered = (lax.all_gather(line, axis), 0, [])
    for a, dim in zip(arrays, dims):
        tiles = lines[:, at : at + a.size].reshape(-1, *a.shape)
        gathered.append(in_order(tiles, dim))
        at += a.size
    return tuple(gathered)


def copy_for_each(value, axis):
    devices = lax.axis_size(axis)
    return lax.all_to_all(
        jnp.broadcast_to(value[None], (devices, *value.shape)), axis, 0, 0, tiled=True
    )


def combined_pairwise(pieces, combine):
    while len(jax.tree.leaves(pieces)[0]) > 1:
        pieces = jax.vmap(combine)(
            *(jax.tree.map(lambda part: part[side::2], pieces) for side in (0, 1))
        )
    return jax.tree.map(lambda part: part[0], pieces)


def carried_in(value, axis, combine, identity, reverse):
    devices, position = (lax.axis_size(axis), lax.axis_index(axis))
    passed = jnp.arange(devices) > position if reverse else jnp.arange(devices) < position

    def kept(part, zero, own):
        part = jnp.where(
            passed.reshape(-1, *(1 for _ in own.shape)),
            part.astype(own.dtype),
            jnp.asarray(zero, own.dtype),
        )
        return part[::-1] if reverse else part

    pieces = jax.tree.map(
        lambda part: copy_for_each(part, axis),
        jax.tree.map(lambda part, kind: part.astype(kind), value, (jnp.bfloat16, jnp.bfloat16)),
    )
    return combined_pairwise(jax.tree.map(kept, pieces, identity, value), combine)


def over_copies(value, axis):
    everything = copy_for_each(value, axis)
    return jnp.sum(everything, axis=0)


def gather_directly(value, axis, dim):
    tiles = copy_for_each(value, axis)
    return in_order(tiles, dim)


def forget_gate_value(gate_logits, gate_lower_limit, surge_decay, head_layout):
    key_gate_random = gate_lower_limit[None, :] * jax.nn.sigmoid(-gate_logits.astype(jnp.float32))
    logarithm_decay = jnp.log1p(-key_gate_random).reshape(head_layout) + surge_decay
    return (key_gate_random.reshape(head_layout), logarithm_decay)


def chain_step(earlier, later_part):
    return (
        earlier[0] + later_part[0],
        jnp.exp(later_part[0])[..., None] * earlier[1] + later_part[1],
    )


def block_pass(queries, key_gate_random, value_rows, logarithm_decay):
    tok_rows, local_heads, channels = queries.shape
    n_blocks = tok_rows // BLOCK
    block_shape = (n_blocks, BLOCK, local_heads, channels)
    queries = queries.reshape(block_shape)
    key_gate_random = key_gate_random.reshape(block_shape)
    value_rows = value_rows.reshape(block_shape)
    running = jnp.cumsum(logarithm_decay.reshape(block_shape), axis=1)
    block_end = running[:, -1]
    query_decay = queries * jnp.exp(running)
    key_rise = key_gate_random * jnp.exp(-running)
    key_tail = key_gate_random * jnp.exp(block_end[:, None] - running)
    scores = jnp.einsum("nthk,nshk->nhts", query_decay, key_rise, precision=top_precision)
    lower_mask = jnp.tril(jnp.ones((BLOCK, BLOCK), dtype=bool))
    scores = jnp.where(lower_mask, scores, 0.0)
    within = jnp.einsum("nhts,nshv->nthv", scores, value_rows, precision=top_precision)
    states = jnp.einsum("nshk,nshv->nhkv", key_tail, value_rows, precision=top_precision)
    prefix_decay, prefix_state = lax.associative_scan(chain_step, (block_end, states), axis=0)
    excl_decay = jnp.concatenate([jnp.zeros_like(block_end[:1]), prefix_decay[:-1]], axis=0)
    excl_state = jnp.concatenate([jnp.zeros_like(states[:1]), prefix_state[:-1]], axis=0)
    return (within, query_decay, excl_decay, excl_state, prefix_decay[-1], prefix_state[-1])


def finish(parts, incoming, head_layout):
    within, query_decay, excl_decay, excl_state = (parts[0], parts[1], parts[2], parts[3])
    start_state = jnp.exp(excl_decay)[..., None] * incoming[None] + excl_state
    result = within + jnp.einsum(
        "nthk,nhkv->nthv", query_decay, start_state, precision=top_precision
    )
    return result.reshape(head_layout)


def per_device(
    residual,
    values,
    forget_onward,
    forget_reverse,
    surge_log_decay,
    gate_limit_complement,
    readout_query,
    output_gate,
    head_norm_gain,
    output_weight,
    mixer_norm_gain,
    up_weight,
    down_weight,
):
    tok_rows = residual.shape[0]
    channels = values.shape[1]
    local_heads = channels // HEAD_DIM
    head_layout = (tok_rows, local_heads, HEAD_DIM)
    up_full, down_full = gather_packed((up_weight, down_weight), "sp", (0, 0))
    queries = (jax.nn.silu(readout_query.astype(jnp.float32)) * HEAD_DIM ** (-0.5)).reshape(
        head_layout
    )
    value_rows = values.astype(jnp.float32).reshape(head_layout)
    surge_decay = surge_log_decay[:, :, None]
    key_onward, logarithm_onward = forget_gate_value(
        forget_onward, gate_limit_complement[0], surge_decay, head_layout
    )
    key_reverse, logarithm_reverse = forget_gate_value(
        forget_reverse, gate_limit_complement[1], surge_decay, head_layout
    )
    fwd_parts = block_pass(queries, key_onward, value_rows, logarithm_onward)
    bwd_parts = block_pass(
        jnp.flip(queries, 0),
        jnp.flip(key_reverse, 0),
        jnp.flip(value_rows, 0),
        jnp.flip(logarithm_reverse, 0),
    )
    zero_decay = jnp.zeros((local_heads, HEAD_DIM), jnp.float32)
    zero_state = jnp.zeros((local_heads, HEAD_DIM, HEAD_DIM), jnp.float32)
    fwd_decay, fwd_state = (fwd_parts[4], fwd_parts[5])
    bwd_decay, bwd_state = (bwd_parts[4], bwd_parts[5])
    fwd_in = carried_in((fwd_decay, fwd_state), "sp", chain_step, (zero_decay, zero_state), False)
    bwd_in = carried_in((bwd_decay, bwd_state), "sp", chain_step, (zero_decay, zero_state), True)
    mixed_out = finish(fwd_parts, fwd_in[1], head_layout) + jnp.flip(
        finish(bwd_parts, bwd_in[1], head_layout), 0
    )
    normed = (
        mixed_out
        * lax.rsqrt(jnp.mean(mixed_out * mixed_out, axis=-1, keepdims=True) + epsilon)
        * head_norm_gain
    )
    gated_rows = (
        normed.reshape(tok_rows, channels) * jax.nn.silu(output_gate.astype(jnp.float32))
    ).astype(jnp.bfloat16)
    partial_value = jnp.dot(gated_rows, output_weight, preferred_element_type=jnp.float32)
    attention = lax.psum_scatter(
        partial_value.astype(jnp.bfloat16), "tp", scatter_dimension=1, tiled=True
    ).astype(jnp.float32)
    middle = (residual.astype(jnp.float32) + attention).astype(jnp.bfloat16)
    own_middle = middle.astype(jnp.float32)
    squares = over_copies(jnp.sum(own_middle * own_middle, axis=1), "tp")
    own_cols = middle.shape[1]
    gain_part = lax.dynamic_slice_in_dim(mixer_norm_gain, lax.axis_index("tp") * own_cols, own_cols)
    scale_rows = lax.rsqrt(squares / D + epsilon)[:, None]
    normalized = (own_middle * scale_rows * gain_part).astype(jnp.bfloat16)
    lifted = jnp.dot(
        gather_directly(normalized, "tp", 1), up_full, preferred_element_type=jnp.float32
    )
    hidden = jnp.square(jax.nn.relu(lifted)).astype(jnp.bfloat16)
    channel_part = lax.dot_general(
        hidden, down_full, (((1,), (1,)), ((), ())), preferred_element_type=jnp.float32
    )
    channel = lax.psum_scatter(
        channel_part.astype(jnp.bfloat16), "tp", scatter_dimension=1, tiled=True
    ).astype(jnp.float32)
    return (own_middle + channel).astype(jnp.bfloat16)


def solution(mesh):
    placed = (
        P("sp", "tp"),
        P("sp", "tp"),
        P("sp", "tp"),
        P("sp", "tp"),
        P("sp", "tp"),
        P(None, "tp"),
        P("sp", "tp"),
        P("sp", "tp"),
        P(),
        P("tp", None),
        P(),
        P("sp", "tp"),
        P("sp", "tp"),
    )
    return jax.shard_map(
        per_device, mesh=mesh, in_specs=placed, out_specs=P("sp", "tp"), check_vma=False
    )
```

profile of v0, /device:TPU:1, one launch (start us, length us, event | category | flops | bytes accessed | tf_op | source)
XLA Modules:
  0.0 495.7 jit_solution(3973693778668981648)
XLA Ops:
  10.9 7.2 %rev.19 = f32[768,2,128]{0,2,1:T(8,128)} reverse(f32[768,2,128]{0,2,1:T(8,128)} %broadcast_add_fusion), dimensions={0} | reverse | bytes 1572864 | tf_op jit(solution)/shard_map/jit(_flip)/rev | solution.py:156
  40.4 8.7 %all-to-all-start.2 = ((bf16[16,2,128]{2,1,0:T(2,128)(2,1)}), bf16[16,2,128]{2,1,0:T(2,128)(2,1)}, u32[]{:S(2)}, u32[]{:S(2)}) async-start(bf16[16,2,128]{2,1,0:T(2,128)(2,1)} %broadcast_in_dim.136), calls=%async_computation.2 | async-start | bytes 16384 | tf_op jit(solution)/shard_map/all_to_all | solution.py:33
  56.9 4.4 rev.18
  64.5 6.7 %rev.21 = f32[768,2,128]{0,2,1:T(8,128)} reverse(bf16[768,2,128]{0,2,1:T(8,128)(2,1)} %bitcast.94), dimensions={0} | reverse | bytes 1179648 | tf_op jit(solution)/shard_map/jit(_flip)/rev | solution.py:155
  93.3 4.9 pad.136
  98.2 5.0 %pad.102 = f32[12,2,128,128]{3,2,1,0:T(8,128)} pad(f32[6,2,128,128]{3,2,1,0:T(8,128)S(1)} %pad_maximum_fusion.2, f32[]{:T(128)} %constant.15.clone.1), padding=0_1_1x0_0_0x0_0_0x0_0_0 | pad | bytes 2359300 | tf_op jit(solution)/shard_map/pad | solution.py:105
  136.9 5.0 %pad.132 = f32[11,2,128,128]{3,2,1,0:T(8,128)} pad(f32[6,2,128,128]{3,2,1,0:T(8,128)S(1)} %pad_maximum_fusion.1, f32[]{:T(128)} %constant.15.clone.1), padding=0_0_1x0_0_0x0_0_0x0_0_0 | pad | bytes 2228228 | tf_op jit(solution)/shard_map/slice | solution.py:107
  141.9 5.0 %pad.90 = f32[12,2,128,128]{3,2,1,0:T(8,128)} pad(f32[6,2,128,128]{3,2,1,0:T(8,128)S(1)} %pad_maximum_fusion.1, f32[]{:T(128)} %constant.15.clone.1), padding=0_1_1x0_0_0x0_0_0x0_0_0 | pad | bytes 2359300 | tf_op jit(solution)/shard_map/pad | solution.py:105
  149.3 8.0 %pad.192 = f32[12,2,128,128]{3,2,1,0:T(8,128)} pad(f32[6,2,128,128]{3,2,1,0:T(8,128)} %add.340, f32[]{:T(128)} %constant.15.clone.1), padding=1_0_1x0_0_0x0_0_0x0_0_0 | pad | bytes 2359300
  162.8 8.0 %pad.195 = f32[12,2,128,128]{3,2,1,0:T(8,128)} pad(f32[6,2,128,128]{3,2,1,0:T(8,128)} %add.310, f32[]{:T(128)} %constant.15.clone.1), padding=1_0_1x0_0_0x0_0_0x0_0_0 | pad | bytes 2359300
  187.3 6.8 %all-to-all-start = ((bf16[16,2,128]{2,1,0:T(2,128)(2,1)}), bf16[16,2,128]{2,1,0:T(2,128)(2,1)}, u32[]{:S(2)}, u32[]{:S(2)}) async-start(bf16[16,2,128]{2,1,0:T(2,128)(2,1)} %broadcast_in_dim.128), calls=%async_computation | async-start | bytes 16384 | tf_op jit(solution)/shard_map/all_to_all | solution.py:33
  210.7 11.1 %all-to-all-done.3 = bf16[16,2,128,128]{3,2,1,0:T(8,128)(2,1)} async-done(((bf16[16,2,128,128]{3,2,1,0:T(8,128)(2,1)}), bf16[16,2,128,128]{3,2,1,0:T(8,128)(2,1)}, u32[]{:S(2)}, u32[]{:S(2)}) %all-to-all-start.3) | async-done | bytes 1048608 | tf_op jit(solution)/shard_map/all_to_all | solution.py:33
  236.0 5.6 %rev.22 = f32[768,2,128]{2,0,1:T(8,128)S(1)} reverse(f32[768,2,128]{2,0,1:T(8,128)} %bitcast.89), dimensions={0} | reverse | bytes 1572864 | tf_op jit(solution)/shard_map/jit(_flip)/rev | solution.py:164
  251.4 4.4 convolution_convert_fusion.1
  258.3 44.0 %reduce-scatter.3.cloned.1.call-done = bf16[768,512]{1,0:T(8,128)(2,1)} async-done(((bf16[768,4096]{1,0:T(8,128)(2,1)}), bf16[768,512]{1,0:T(8,128)(2,1)}) %reduce-scatter.3.cloned.1.call-update) | async-done | bytes 786448 | tf_op jit(solution)/shard_map/reduce_scatter | solution.py:176
  304.6 5.0 %all-to-all-start.4 = ((f32[8,1,768]{2,1,0:T(1,128)}), f32[8,1,768]{2,1,0:T(1,128)S(1)}, u32[]{:S(2)}, u32[]{:S(2)}) async-start(f32[8,1,768]{2,1,0:T(1,128)} %broadcast_in_dim.140), calls=%async_computation.5 | async-start | bytes 49152 | tf_op jit(solution)/shard_map/all_to_all | solution.py:33
  318.0 5.4 %all-to-all-start.5 = ((bf16[8,768,512]{1,2,0:T(8,128)(2,1)}), bf16[8,768,512]{1,2,0:T(8,128)(2,1)}, u32[]{:S(2)}, u32[]{:S(2)}) async-start(bf16[8,768,512]{1,2,0:T(8,128)(2,1)} %broadcast_in_dim.141), calls=%async_computation.6 | async-start | bytes 12582912 | tf_op jit(solution)/shard_map/all_to_all | solution.py:33
  323.4 50.4 %all-gather.3.cloned.1.call-done = bf16[8388608]{0:T(1024)(128)(2,1)} async-done(((bf16[524288]{0:T(1024)(128)(2,1)}), bf16[8388608]{0:T(1024)(128)(2,1)}) %all-gather.3.cloned.1.call-update) | async-done | bytes 16777232 | tf_op jit(solution)/shard_map/all_gather | solution.py:23
  373.8 20.5 %reshape.149 = bf16[16,524288]{1,0:T(8,128)(2,1)} reshape(bf16[8388608]{0:T(1024)(128)(2,1)} %all-gather.3.cloned.1.call-done) | data formatting | bytes 33554432 | tf_op jit(solution)/shard_map/all_gather | solution.py:23
  394.3 11.4 %fusion.75 = (bf16[16,262144]{1,0:T(8,128)(2,1)}, bf16[16,262144]{1,0:T(8,128)(2,1)}) fusion(bf16[16,524288]{1,0:T(8,128)(2,1)} %reshape.149), kind=kLoop, calls=%fused_computation.187 | loop fusion | bytes 33554432 | tf_op jit(solution)/shard_map/slice | solution.py:25
  405.7 8.0 %reshape_reshape.19 = bf16[4096,1024]{1,0:T(8,128)(2,1)} reshape(bf16[16,262144]{1,0:T(8,128)(2,1)} %get-tuple-element.14) | data formatting | bytes 16777216 | tf_op jit(solution)/shard_map/reshape;reshape | solution.py:18
  413.7 7.9 %reshape_reshape.18 = bf16[4096,1024]{1,0:T(8,128)(2,1)} reshape(bf16[16,262144]{1,0:T(8,128)(2,1)} %get-tuple-element.13) | data formatting | bytes 16777216 | tf_op jit(solution)/shard_map/reshape;reshape | solution.py:18
  421.6 22.0 %convolution_convert_fusion = bf16[768,4096]{1,0:T(8,128)(2,1)} fusion(bf16[4096,1024]{1,0:T(8,128)(2,1)} %reshape_reshape.19, bf16[768,4096]{0,1:T(8,128)(2,1)} %bitcast.33, bf16[4096,1024]{1,0:T(8,128)(2,1)} %reshape_reshape.18), kind=kOutput, calls=%fused_computation | convolution fusion | flops 12890406912 | bytes 29360128 | tf_op jit(solution)/shard_map/dot_general | solution.py:190
  443.6 41.9 %reduce-scatter.5.cloned.1.call-done = bf16[768,512]{1,0:T(8,128)(2,1)} async-done(((bf16[768,4096]{1,0:T(8,128)(2,1)}), bf16[768,512]{1,0:T(8,128)(2,1)}) %reduce-scatter.5.cloned.1.call-update) | async-done | bytes 786448 | tf_op jit(solution)/shard_map/reduce_scatter | solution.py:193
  (336 shorter events, 172.3 us)
Async XLA Ops:
  7.4 244.0 %copy-start = (bf16[256,4096]{1,0:T(8,128)(2,1)S(1)}, bf16[256,4096]{1,0:T(8,128)(2,1)}, u32[]{:S(2)}) copy-start(bf16[256,4096]{1,0:T(8,128)(2,1)} %param.22) | copy-start | bytes 6291460
  36.6 19.8 %copy-start.44 = (f32[6,2,128]{2,0,1:T(8,128)}, f32[6,2,128]{2,0,1:T(8,128)S(1)}, u32[]{:S(2)}) copy-start(f32[6,2,128]{2,0,1:T(8,128)S(1)} %pad.95) | copy-start | bytes 18436
  36.7 19.8 %copy-start.46 = (f32[6,2,128]{2,0,1:T(8,128)}, f32[6,2,128]{2,0,1:T(8,128)S(1)}, u32[]{:S(2)}) copy-start(f32[6,2,128]{2,0,1:T(8,128)S(1)} %pad.94) | copy-start | bytes 18436
  38.6 17.9 %copy-start.42 = (f32[6,2,128]{2,0,1:T(8,128)}, f32[6,2,128]{2,0,1:T(8,128)S(1)}, u32[]{:S(2)}) copy-start(f32[6,2,128]{2,0,1:T(8,128)S(1)} %pad.83) | copy-start | bytes 18436
  39.1 17.3 %copy-start.36 = (f32[6,2,128]{2,0,1:T(8,128)}, f32[6,2,128]{2,0,1:T(8,128)S(1)}, u32[]{:S(2)}) copy-start(f32[6,2,128]{2,0,1:T(8,128)S(1)} %add.298) | copy-start | bytes 18436
  39.2 17.3 %copy-start.38 = (f32[6,2,128]{2,0,1:T(8,128)}, f32[6,2,128]{2,0,1:T(8,128)S(1)}, u32[]{:S(2)}) copy-start(f32[6,2,128]{2,0,1:T(8,128)S(1)} %add.328) | copy-start | bytes 18436
  40.4 146.3 %all-to-all-start.2 = ((bf16[16,2,128]{2,1,0:T(2,128)(2,1)}), bf16[16,2,128]{2,1,0:T(2,128)(2,1)}, u32[]{:S(2)}, u32[]{:S(2)}) async-start(bf16[16,2,128]{2,1,0:T(2,128)(2,1)} %broadcast_in_dim.136), calls=%async_computation.2 | async-start | bytes 16384 | tf_op jit(solution)/shard_map/all_to_all | solution.py:33
  56.9 6.7 %copy-start.6 = (f32[768,256]{0,1:T(8,128)}, f32[768,256]{0,1:T(8,128)S(1)}, u32[]{:S(2)}) copy-start(f32[768,256]{0,1:T(8,128)S(1)} %fusion.28) | copy-start | bytes 2359300
  56.9 6.7 %copy-start.30 = (bf16[768,256]{1,0:T(8,128)(2,1)S(1)}, bf16[768,256]{1,0:T(8,128)(2,1)}, u32[]{:S(2)}) copy-start(bf16[768,256]{1,0:T(8,128)(2,1)} %param.14) | copy-start | bytes 1179652
  103.2 7.1 %copy-start.27 = (f32[768,256]{0,1:T(8,128)S(1)}, f32[768,256]{0,1:T(8,128)}, u32[]{:S(2)}) copy-start(f32[768,256]{0,1:T(8,128)} %get-tuple-element.24) | copy-start | bytes 2359300
  109.6 11.2 %copy-start.24 = (bf16[12,64,2,128]{3,2,1,0:T(2,128)(2,1)}, bf16[12,64,2,128]{3,2,1,0:T(2,128)(2,1)S(1)}, u32[]{:S(2)}) copy-start(bf16[12,64,2,128]{3,2,1,0:T(2,128)(2,1)S(1)} %reshape_reshape.17) | copy-start | bytes 1179652
  146.9 10.4 %copy-start.18 = (f32[11,2,128,128]{3,2,1,0:T(8,128)S(1)}, f32[11,2,128,128]{3,2,1,0:T(8,128)}, u32[]{:S(2)}) copy-start(f32[11,2,128,128]{3,2,1,0:T(8,128)} %pad.136) | copy-start | bytes 4325380
  187.3 13.1 %all-to-all-start = ((bf16[16,2,128]{2,1,0:T(2,128)(2,1)}), bf16[16,2,128]{2,1,0:T(2,128)(2,1)}, u32[]{:S(2)}, u32[]{:S(2)}) async-start(bf16[16,2,128]{2,1,0:T(2,128)(2,1)} %broadcast_in_dim.128), calls=%async_computation | async-start | bytes 16384 | tf_op jit(solution)/shard_map/all_to_all | solution.py:33
  202.5 19.2 %all-to-all-start.3 = ((bf16[16,2,128,128]{3,2,1,0:T(8,128)(2,1)}), bf16[16,2,128,128]{3,2,1,0:T(8,128)(2,1)}, u32[]{:S(2)}, u32[]{:S(2)}) async-start(bf16[16,2,128,128]{3,2,1,0:T(8,128)(2,1)} %broadcast_in_dim.139), calls=%async_computation.3 | async-start | bytes 2097152 | tf_op jit(solution)/shard_map/all_to_all | solution.py:33
  223.8 18.1 %all-to-all-start.1 = ((bf16[16,2,128,128]{3,2,1,0:T(8,128)(2,1)}), bf16[16,2,128,128]{3,2,1,0:T(8,128)(2,1)}, u32[]{:S(2)}, u32[]{:S(2)}) async-start(bf16[16,2,128,128]{3,2,1,0:T(8,128)(2,1)} %broadcast_in_dim.132), calls=%async_computation.1 | async-start | bytes 2097152 | tf_op jit(solution)/shard_map/all_to_all | solution.py:33
  228.2 74.1 %reduce-scatter.3.cloned.1.call-start = ((), (), s32[]{:S(2)}) async-start(), calls=%async_computation.8 | async-start | bytes 7077888 | tf_op jit(solution)/shard_map/reduce_scatter | solution.py:176
  235.1 6.8 %copy-start.65 = (pred[16]{0:T(512)(128)(4,1)S(1)}, pred[16]{0:T(512)(128)(4,1)}, u32[]{:S(2)}) copy-start(pred[16]{0:T(512)(128)(4,1)} %iota_compare_fusion.2) | copy-start | bytes 52
  255.8 117.9 %all-gather.3.cloned.1.call-start = ((), (), s32[]{:S(2)}) async-start(), calls=%async_computation.10 | async-start | bytes 17825792 | tf_op jit(solution)/shard_map/all_gather | solution.py:23
  257.1 45.1 %copy-start.7 = (bf16[768,512]{1,0:T(8,128)(2,1)S(1)}, bf16[768,512]{1,0:T(8,128)(2,1)}, u32[]{:S(2)}) copy-start(bf16[768,512]{1,0:T(8,128)(2,1)} %param.13) | copy-start | bytes 2359300
  302.2 12.1 %copy-start.10 = (bf16[768,512]{1,0:T(8,128)(2,1)S(1)}, bf16[768,512]{1,0:T(8,128)(2,1)}, u32[]{:S(2)}) copy-start(bf16[768,512]{1,0:T(8,128)(2,1)} %reduce-scatter.3.cloned.1.call-done) | copy-start | bytes 2359300
  304.6 9.8 %all-to-all-start.4 = ((f32[8,1,768]{2,1,0:T(1,128)}), f32[8,1,768]{2,1,0:T(1,128)S(1)}, u32[]{:S(2)}, u32[]{:S(2)}) async-start(f32[8,1,768]{2,1,0:T(1,128)} %broadcast_in_dim.140), calls=%async_computation.5 | async-start | bytes 49152 | tf_op jit(solution)/shard_map/all_to_all | solution.py:33
  318.0 103.6 %all-to-all-start.5 = ((bf16[8,768,512]{1,2,0:T(8,128)(2,1)}), bf16[8,768,512]{1,2,0:T(8,128)(2,1)}, u32[]{:S(2)}, u32[]{:S(2)}) async-start(bf16[8,768,512]{1,2,0:T(8,128)(2,1)} %broadcast_in_dim.141), calls=%async_computation.6 | async-start | bytes 12582912 | tf_op jit(solution)/shard_map/all_to_all | solution.py:33
  323.4 162.1 %reduce-scatter.5.cloned.1.call-start = ((), (), s32[]{:S(2)}) async-start(), calls=%async_computation.9 | async-start | bytes 7077888 | tf_op jit(solution)/shard_map/reduce_scatter | solution.py:193
  443.6 44.5 %copy-start.1 = (bf16[256,4096]{1,0:T(8,128)(2,1)S(1)}, bf16[256,4096]{1,0:T(8,128)(2,1)}, u32[]{:S(2)}) copy-start(bf16[256,4096]{1,0:T(8,128)(2,1)} %param.22) | copy-start | bytes 6291460
  (56 other events, 146.5 us)
Sparse Core Ops, SparseCore 0:
  256.0 46.2 reduce-scatter.2
  443.7 41.7 reduce-scatter.4
Sparse Core Ops, SparseCore 1:
  258.5 115.3 all-gather.2
where the time goes:
time: 505 us; the launch traced here: 496 us
  local copies, waits for them, and re-layouts  187 us (37%)
  waiting for transfers between devices  155 us (31%)
  other arithmetic  59.8 us (12%)
  matrix products  42.5 us (8%)
  starting transfers between devices  34.6 us (7%)
  between operations  16.2 us (3%)
    all_gather x1, waiting for transfers between devices, gather_packed(): lines, at, gathered = (lax.all_gather(line, axis), 0, [])  50.4 us
    reduce_scatter x1, waiting for transfers between devices, per_device(): lax.psum_scatter(partial_value.astype(jnp.bfloat16), 'tp', scatter_dimens...  44 us
    reduce_scatter x1, waiting for transfers between devices, per_device(): lax.psum_scatter(channel_part.astype(jnp.bfloat16), 'tp', scatter_dimensi...  41.9 us
    all_to_all x6, starting transfers between devices, copy_for_each(): lax.all_to_all(jnp.broadcast_to(value[None], (devices, *value.shape)), ax...  34.5 us
    unnamed x147, local copies, waits for them, and re-layouts  30 us
    pad x18, local copies, waits for them, and re-layouts, block_pass(): lax.associative_scan(chain_step, (block_end, states), axis=0)  23.8 us
    dot_general x1, matrix products, per_device(): lax.dot_general(hidden, down_full, (((1,), (1,)), ((), ())), preferred_el...  22 us
    all_gather x1, local copies, waits for them, and re-layouts, gather_packed(): lines, at, gathered = (lax.all_gather(line, axis), 0, [])  20.5 us
  transfers between devices with their start and end apart: 9, of which 7 were waited for; matrix products, arithmetic and copies ran while one was open for 42% of the time, Pallas kernels for 0%

commit v1 on v0

v1 whole, which is shorter than its diff:
```python
import functools

import jax
import jax.numpy as jnp
from jax import lax
from jax.experimental import pallas as pl
from jax.experimental.pallas import tpu as pltpu
from jax.sharding import PartitionSpec as P

D = 4096
HD = 128
HEADS = 2
CH = HEADS * HD
TOK = 768
BLK = 64
NB = TOK // BLK
OC = 512
FFL = 1024
SHARD = 256
QUARTER = 64
EPS = 1e-06
MESH = pl.DeviceIdType.MESH
F32 = jnp.float32
BF16 = jnp.bfloat16
ST_ROWS = 272


def dot(a, b, dims=(((1,), (0,)), ((), ()))):
    return lax.dot_general(a, b, dims, preferred_element_type=F32)


LAST = (((1,), (1,)), ((), ()))
FIRST = (((0,), (0,)), ((), ()))


def sigmoid(x):
    return 1.0 / (1.0 + jnp.exp(-x))


def kernel(
    residual, values, f_on, f_rev, surge, glc, query, gate, head_gain, out_w,
    norm_gain, up_w, down_w,
    out,
    res_v, val_v, fon_v, frev_v, sur_v, glc_v, que_v, gat_v, hg_v, ng_v,
    wu, wd, owc, ga, xa,
    qd, kr, sx, em, elx, run_state, run_log, st, st_in, sin, o_v, att,
    xg, ss, acc, hid,
    d2s, d2r, cs, ra, e1, e2,
    in_sem, w_send, w_recv, ow_send, ow_recv, st_send, st_recv,
    g_send, g_recv, x_send, x_recv, c_send, c_recv, r_send, r_recv, e_send, e_recv,
):
    sp, tp = lax.axis_index("sp"), lax.axis_index("tp")
    x, z = lax.rem(sp, 4), lax.div(sp, 4)
    core, y = lax.rem(tp, 2), lax.div(tp, 2)
    other = 1 - core

    def ring(v, k):
        return lax.rem(v + (k % 4), 4)

    yp, ym, y2 = ring(y, 1), ring(y, 3), ring(y, 2)
    partner = 2 * y + other

    barrier = pltpu.get_barrier_semaphore()
    for o in range(1, 16):
        pl.semaphore_signal(barrier, inc=1, device_id=(lax.rem(sp + o, 16), tp), device_id_type=MESH)
    for o in range(1, 8):
        pl.semaphore_signal(barrier, inc=1, device_id=(sp, lax.rem(tp + o, 8)), device_id_type=MESH)

    own_rows = pl.ds(pl.multiple_of(sp * SHARD, SHARD), SHARD)
    ow_rows = pl.ds(pl.multiple_of(tp * 256, 256), 256)
    own_cols = pl.ds(pl.multiple_of(tp * OC, OC), OC)
    loads = [
        (f_on, fon_v), (f_rev, frev_v), (surge, sur_v), (glc, glc_v), (query, que_v),
        (values, val_v), (gate, gat_v), (head_gain, hg_v), (residual, res_v), (norm_gain, ng_v),
        (up_w, wu.at[own_rows]), (down_w, wd.at[own_rows]),
        (out_w.at[:, own_cols], owc.at[ow_rows]),
    ]
    loads = [pltpu.make_async_copy(a, b, in_sem.at[i]) for i, (a, b) in enumerate(loads)]
    for copy in loads:
        copy.start()

    pl.semaphore_wait(barrier, 22)

    def remote(src, dst, ss_, rs_, dev):
        return pltpu.make_async_remote_copy(
            src_ref=src, dst_ref=dst, send_sem=ss_, recv_sem=rs_, device_id=dev, device_id_type=MESH
        )

    started = []

    def send(*args):
        copy = remote(*args)
        copy.start()
        started.append(copy)

    weights = ((up_w, wu), (down_w, wd))

    def sp_at(half, i, j):
        return ring(z, j) * 4 + ring(x, i) if half == 0 else ring(z, i) * 4 + ring(x, j)

    def piece(t, half, i, j, part):
        start, size = (0, 2 * QUARTER) if part is None else (part * QUARTER, QUARTER)
        first = sp_at(half, i, j) * SHARD + half * 2 * QUARTER + start
        return weights[t][1].at[pl.ds(pl.multiple_of(first, QUARTER), size)]

    FWD = (0, -1, 1, 2)

    def w_copy(t, half, slot, i, j, part, to, src=None):
        ref = piece(t, half, i, j, part)
        return remote(
            ref if src is None else src, ref, w_send.at[t, half, slot], w_recv.at[t, half, slot],
            (sp_at(half, *to), tp),
        )

    def w_go(*args, **kw):
        copy = w_copy(*args, **kw)
        copy.start()
        started.append(copy)

    def w_got(t, half, slot, i, j, part):
        w_copy(t, half, slot, i, j, part, (1, 0)).wait_recv()

    def w_second(t, half, n, src=None):
        i = FWD[n]
        w_go(t, half, 4 + 4 * n, i, 0, None, (0, 1), src=src)
        w_go(t, half, 5 + 4 * n, i, 0, None, (0, -1), src=src)

    def w_second_forward(t, half, n):
        i = FWD[n]
        w_got(t, half, 4 + 4 * n, i, -1, None)
        w_go(t, half, 6 + 4 * n, i, -1, 0, (0, 1))
        w_got(t, half, 5 + 4 * n, i, 1, None)
        w_go(t, half, 7 + 4 * n, i, 1, 1, (0, -1))

    def level0(t):
        for half in range(2):
            src = weights[t][0].at[pl.ds(half * 2 * QUARTER, 2 * QUARTER)]
            w_go(t, half, 0, 0, 0, None, (1, 0), src=src)
            w_go(t, half, 1, 0, 0, None, (-1, 0), src=src)
        for half in range(2):
            src = weights[t][0].at[pl.ds(half * 2 * QUARTER, 2 * QUARTER)]
            w_second(t, half, 0, src=src)

    def level1(t):
        for half in range(2):
            w_got(t, half, 0, -1, 0, None)
            w_go(t, half, 2, -1, 0, 0, (1, 0))
            w_got(t, half, 1, 1, 0, None)
            w_go(t, half, 3, 1, 0, 1, (-1, 0))
        for half in range(2):
            w_second(t, half, 1)
            w_second(t, half, 2)
        for half in range(2):
            w_second_forward(t, half, 0)

    def level2(t):
        for half in range(2):
            w_got(t, half, 2, 2, 0, 0)
            w_got(t, half, 3, 2, 0, 1)
            w_second(t, half, 3)
        for half in range(2):
            w_second_forward(t, half, 1)
            w_second_forward(t, half, 2)

    def level3(t):
        for half in range(2):
            w_second_forward(t, half, 3)

    def level4(t):
        for half in range(2):
            for n in range(4):
                w_got(t, half, 6 + 4 * n, FWD[n], 2, 0)
                w_got(t, half, 7 + 4 * n, FWD[n], 2, 1)

    level0(0)

    def ow_copy(o):
        to = lax.rem(tp + o, 8)
        return remote(
            out_w.at[:, pl.ds(pl.multiple_of(to * OC, OC), OC)], owc.at[ow_rows],
            ow_send.at[o - 1], ow_recv.at[o - 1], (sp, to),
        )

    for o in range(1, 8):
        copy = ow_copy(o)
        copy.start()
        started.append(copy)

    for copy in loads[:7]:
        copy.wait()

    row_id = lax.broadcasted_iota(jnp.int32, (BLK, BLK), 0)
    col_id = lax.broadcasted_iota(jnp.int32, (BLK, BLK), 1)
    lower, upper = row_id >= col_id, row_id <= col_id
    run_state[...] = jnp.zeros_like(run_state)
    run_log[...] = jnp.zeros_like(run_log)

    def pass1(step, carry):
        for d, (logits, tri, mid_at, end_at) in enumerate(
            ((fon_v, lower, BLK // 2 - 1, BLK - 1), (frev_v, upper, BLK // 2, 0))
        ):
            blk = step if d == 0 else NB - 1 - step
            rows = pl.ds(pl.multiple_of(blk * BLK, BLK), BLK)
            key = glc_v[d : d + 1, :] / (1.0 + jnp.exp(logits[rows, :].astype(F32)))
            sg = sur_v[rows, :]
            sg = jnp.concatenate(
                [jnp.broadcast_to(sg[:, h : h + 1], (BLK, HD)) for h in range(HEADS)], axis=1
            )
            logs = jnp.log1p(-key) + sg
            run = lax.dot_general(
                jnp.where(tri, 1.0, 0.0).astype(F32), logs, (((1,), (0,)), ((), ())),
                precision=lax.Precision.HIGHEST, preferred_element_type=F32,
            )
            mid, end = run[mid_at : mid_at + 1, :], run[end_at : end_at + 1, :]
            q = que_v[rows, :].astype(F32)
            q = q * sigmoid(q) * (HD ** -0.5)
            qd[d, rows, :] = (q * jnp.exp(run - mid)).astype(BF16)
            k = key * jnp.exp(mid - run)
            kr[d, rows, :] = k.astype(BF16)
            tail = (k * jnp.exp(end - mid)).astype(BF16)
            v = val_v[rows, :]
            gone = run_log[d, 0:1, :]
            em[d, blk] = jnp.broadcast_to(jnp.exp(mid), (8, CH))
            elx[d, blk] = jnp.broadcast_to(jnp.exp(gone), (8, CH))
            run_log[d] = jnp.broadcast_to(gone + end, (8, CH))
            decay = jnp.exp(end)
            for h in range(HEADS):
                hs = slice(h * HD, (h + 1) * HD)
                state = run_state[d, hs, :]
                sx[d, blk, hs, :] = state.astype(BF16)
                run_state[d, hs, :] = state * decay[:, hs] + dot(v[:, hs], tail[:, hs], FIRST)
        return carry

    lax.fori_loop(0, NB, pass1, 0)

    for d in range(2):
        st[d, 0:CH, :] = run_state[d].astype(BF16)
        total = run_log[d, 0:1, :]
        high = total.astype(BF16).astype(F32)
        low = total - high
        st[d, CH:ST_ROWS, :] = jnp.concatenate(
            [high[:, :HD], high[:, HD:], low[:, :HD], low[:, HD:], jnp.zeros((12, HD), F32)], axis=0
        ).astype(BF16)

    def st_copy(o):
        return remote(
            st.at[lax.div(sp + o, 16)], st_in.at[o - 1], st_send.at[o - 1], st_recv.at[o - 1],
            (lax.rem(sp + o, 16), tp),
        )

    for o in range(1, 16):
        copy = st_copy(o)
        copy.start()
        started.append(copy)

    def pass2(blk, carry):
        rows = pl.ds(pl.multiple_of(blk * BLK, BLK), BLK)
        v = val_v[rows, :]
        for h in range(HEADS):
            hs = slice(h * HD, (h + 1) * HD)
            fwd = dot(qd[0, rows, hs], kr[0, rows, hs], LAST)
            bwd = dot(qd[1, rows, hs], kr[1, rows, hs], LAST)
            score = jnp.where(lower, fwd, 0.0) + jnp.where(upper, bwd, 0.0)
            o_v[rows, hs] = dot(score.astype(BF16), v[:, hs])
        return carry

    lax.fori_loop(0, NB, pass2, 0)

    level1(0)
    level0(1)

    sin[...] = jnp.zeros_like(sin)
    for o in range(1, 16):
        st_copy(o).wait_recv()

    def combine(i, carry):
        d = lax.div(i + 16 - sp, 16)
        slot = (1 - d) * (sp - 1 - i) + d * i
        tail = st_in[slot, CH:ST_ROWS, :].astype(F32)
        for h in range(HEADS):
            hs = slice(h * HD, (h + 1) * HD)
            decay = jnp.exp(tail[h : h + 1, :] + tail[2 + h : 3 + h, :])
            sin[d, hs, :] = sin[d, hs, :] * decay + st_in[slot, hs, :].astype(F32)
        return carry

    lax.fori_loop(0, 15, combine, 0)

    for copy in loads[6:10]:
        if copy is not loads[6]:
            copy.wait()

    def pass3(blk, carry):
        rows = pl.ds(pl.multiple_of(blk * BLK, BLK), BLK)
        for h in range(HEADS):
            hs = slice(h * HD, (h + 1) * HD)
            mixed = o_v[rows, hs]
            for d in range(2):
                qs = (qd[d, rows, hs].astype(F32) * em[d, blk, 0:1, hs]).astype(BF16)
                state = sx[d, blk, hs, :].astype(F32) + elx[d, blk, 0:1, hs] * sin[d, hs, :]
                mixed = mixed + dot(qs, state.astype(BF16), LAST)
            norm = mixed * lax.rsqrt(jnp.mean(mixed * mixed, axis=-1, keepdims=True) + EPS)
            g = gat_v[rows, hs].astype(F32)
            ga[tp, rows, hs] = (norm * hg_v[0:1, :] * (g * sigmoid(g))).astype(BF16)
        return carry

    lax.fori_loop(0, NB, pass3, 0)

    HALF = TOK // 2

    class Gather:
        def __init__(self, buf, send_sem, recv_sem):
            self.buf, self.ss, self.rs = buf, send_sem, recv_sem

        def copy(self, k, slot, part, to):
            ref = self.buf.at[slot]
            if part is not None:
                ref = self.buf.at[slot, pl.ds(part * HALF, HALF)]
            return remote(ref, ref, self.ss.at[k], self.rs.at[k], (sp, to))

        def go(self, *args):
            copy = self.copy(*args)
            copy.start()
            started.append(copy)

        def got(self, k, slot, part):
            self.copy(k, slot, part, partner).wait_recv()

        def own(self):
            self.go(0, tp, None, 2 * yp + core)
            self.go(1, tp, None, 2 * ym + core)
            self.go(4, tp, None, partner)

        def from_side(self):
            left, right = 2 * ym + core, 2 * yp + core
            self.got(0, left, None)
            self.go(2, left, 0, right)
            self.go(5, left, None, partner)
            self.got(1, right, None)
            self.go(3, right, 1, left)
            self.go(6, right, None, partner)

        def from_far(self):
            far = 2 * y2 + core
            self.got(2, far, 0)
            self.go(7, far, 0, partner)
            self.got(3, far, 1)
            self.go(8, far, 1, partner)

    gathered = Gather(ga, g_send, g_recv)
    gathered.own()

    for copy in loads[10:13]:
        copy.wait()
    for o in range(1, 8):
        ow_copy(o).wait_recv()

    def project(block, first=False):
        def tile(n, carry):
            cols = pl.ds(pl.multiple_of(n * 256, 256), 256)
            part = dot(ga[block], owc[pl.ds(pl.multiple_of(block * 256, 256), 256), cols])
            att[:, cols] = part if first else att[:, cols] + part
            return carry

        lax.fori_loop(0, OC // 256, tile, 0)

    project(tp, True)
    gathered.got(4, partner, None)
    project(partner)
    gathered.from_side()
    project(2 * ym + core)
    project(2 * yp + core)
    level2(0)
    level1(1)
    gathered.got(5, 2 * ym + other, None)
    project(2 * ym + other)
    gathered.got(6, 2 * yp + other, None)
    project(2 * yp + other)
    gathered.from_far()
    project(2 * y2 + core)
    gathered.got(7, 2 * y2 + other, 0)
    gathered.got(8, 2 * y2 + other, 1)
    project(2 * y2 + other)

    TILE = 128

    def middle(i, carry):
        rows = pl.ds(pl.multiple_of(i * TILE, TILE), TILE)
        xa[tp, rows, :] = (res_v[rows, :].astype(F32) + att[rows, :]).astype(BF16)
        return carry

    lax.fori_loop(0, TOK // TILE, middle, 0)

    spread = Gather(xa, x_send, x_recv)
    spread.own()
    level3(0)
    level2(1)
    level4(0)

    def lift(block, first=False):
        gain = ng_v[pl.ds(block, 1), :]

        def scale(i, carry):
            rows = pl.ds(pl.multiple_of(i * TILE, TILE), TILE)
            v = xa[block, rows, :].astype(F32)
            sq = v * v
            sq = (sq[:, 0:128] + sq[:, 128:256]) + (sq[:, 256:384] + sq[:, 384:512])
            ss[rows, :] = sq if first else ss[rows, :] + sq
            xg[rows, :] = (v * gain).astype(BF16)
            return carry

        lax.fori_loop(0, TOK // TILE, scale, 0)

        def tile(n, carry):
            cols = pl.ds(pl.multiple_of(n * 256, 256), 256)
            part = dot(xg[...], wu[pl.ds(pl.multiple_of(block * OC, OC), OC), cols])
            acc[:, cols] = part if first else acc[:, cols] + part
            return carry

        lax.fori_loop(0, FFL // 256, tile, 0)

    lift(tp, True)
    spread.got(4, partner, None)
    lift(partner)
    spread.from_side()
    lift(2 * ym + core)
    lift(2 * yp + core)
    spread.got(5, 2 * ym + other, None)
    lift(2 * ym + other)
    spread.got(6, 2 * yp + other, None)
    lift(2 * yp + other)
    spread.from_far()
    lift(2 * y2 + core)
    spread.got(7, 2 * y2 + other, 0)
    spread.got(8, 2 * y2 + other, 1)
    lift(2 * y2 + other)

    def activate(i, carry):
        rows = pl.ds(pl.multiple_of(i * TILE, TILE), TILE)
        total = jnp.sum(ss[rows, :], axis=-1, keepdims=True)
        v = jnp.maximum(acc[rows, :] * lax.rsqrt(total / D + EPS), 0.0)
        hid[rows, :] = (v * v).astype(BF16)
        return carry

    lax.fori_loop(0, TOK // TILE, activate, 0)

    level3(1)
    level4(1)

    def down(dest, to_ref):
        def tile(n, carry):
            cols = pl.ds(pl.multiple_of(n * 256, 256), 256)
            first = pl.multiple_of(dest * OC + n * 256, 256)
            to_ref[:, cols] = dot(hid[...], wd[pl.ds(first, 256), :], LAST).astype(BF16)
            return carry

        lax.fori_loop(0, OC // 256, tile, 0)

    def c_copy(n):
        return remote(d2s.at[n], d2r.at[n], c_send.at[n], c_recv.at[n], (sp, partner))

    def chip_sum(n):
        c_copy(n).wait_recv()

        def add(i, carry):
            rows = pl.ds(pl.multiple_of(i * TILE, TILE), TILE)
            cs[n, rows, :] = (cs[n, rows, :].astype(F32) + d2r[n, rows, :].astype(F32)).astype(BF16)
            return carry

        lax.fori_loop(0, TOK // TILE, add, 0)

    dests = (y2, yp, ym, y)

    def pair(n):
        down(2 * dests[n] + other, d2s.at[n])
        copy = c_copy(n)
        copy.start()
        started.append(copy)
        down(2 * dests[n] + core, cs.at[n])

    low, high = pl.ds(0, HALF), pl.ds(HALF, HALF)
    right, left = (sp, 2 * yp + core), (sp, 2 * ym + core)

    def r_copy(k):
        half, to = ((low, right), (high, left))[k]
        return remote(cs.at[0, half], ra.at[k], r_send.at[k], r_recv.at[k], to)

    def e_copy(k):
        n, buf, half, to = (
            (1, e1, high, right), (2, e2, low, left), (1, e1, low, right), (2, e2, high, left)
        )[k]
        return remote(cs.at[n, half], buf.at[half], e_send.at[k], e_recv.at[k], to)

    def go(copy):
        copy.start()
        started.append(copy)

    pair(0)
    pair(1)
    chip_sum(0)
    go(r_copy(0))
    go(r_copy(1))
    pair(2)
    chip_sum(1)
    go(e_copy(0))
    chip_sum(2)
    go(e_copy(1))
    pair(3)

    def join(k):
        r_copy(k).wait_recv()
        n = 1 + k

        def add(i, carry):
            rows = pl.ds(pl.multiple_of(k * HALF + i * TILE, TILE), TILE)
            got = ra[k, pl.ds(pl.multiple_of(i * TILE, TILE), TILE), :]
            cs[n, rows, :] = (cs[n, rows, :].astype(F32) + got.astype(F32)).astype(BF16)
            return carry

        lax.fori_loop(0, HALF // TILE, add, 0)

    join(0)
    go(e_copy(2))
    join(1)
    go(e_copy(3))

    c_copy(3).wait_recv()
    for k in range(4):
        e_copy(k).wait_recv()

    def finish(i, carry):
        rows = pl.ds(pl.multiple_of(i * TILE, TILE), TILE)
        total = cs[3, rows, :].astype(F32) + d2r[3, rows, :].astype(F32)
        total = total + (e1[rows, :].astype(F32) + e2[rows, :].astype(F32))
        res_v[rows, :] = (xa[tp, rows, :].astype(F32) + total).astype(BF16)
        return carry

    lax.fori_loop(0, TOK // TILE, finish, 0)
    final = pltpu.make_async_copy(res_v, out, in_sem.at[0])
    final.start()
    for copy in started:
        copy.wait_send()
    final.wait()


def per_device(
    residual, values, forget_onward, forget_reverse, surge_log_decay, gate_limit_complement,
    readout_query, output_gate, head_norm_gain, output_weight, mixer_norm_gain, up_weight,
    down_weight,
):
    any_spec = pl.BlockSpec(memory_space=pl.ANY)
    vmem, dma = pltpu.VMEM, pltpu.SemaphoreType.DMA
    scratch = [
        vmem((TOK, OC), BF16), vmem((TOK, CH), BF16), vmem((TOK, CH), BF16), vmem((TOK, CH), BF16),
        vmem((TOK, HEADS), F32), vmem((2, CH), F32), vmem((TOK, CH), BF16), vmem((TOK, CH), BF16),
        vmem((1, HD), F32), vmem((8, OC), F32),
        vmem((D, FFL), BF16), vmem((D, FFL), BF16), vmem((2048, OC), BF16),
        vmem((8, TOK, CH), BF16), vmem((8, TOK, OC), BF16),
        vmem((2, TOK, CH), BF16), vmem((2, TOK, CH), BF16), vmem((2, NB, CH, HD), BF16),
        vmem((2, NB, 8, CH), F32), vmem((2, NB, 8, CH), F32),
        vmem((2, CH, HD), F32), vmem((2, 8, CH), F32),
        vmem((2, ST_ROWS, HD), BF16), vmem((15, ST_ROWS, HD), BF16), vmem((2, CH, HD), F32),
        vmem((TOK, CH), F32), vmem((TOK, OC), F32),
        vmem((TOK, OC), BF16), vmem((TOK, HD), F32), vmem((TOK, FFL), F32), vmem((TOK, FFL), BF16),
        vmem((4, TOK, OC), BF16), vmem((4, TOK, OC), BF16), vmem((4, TOK, OC), BF16),
        vmem((2, TOK // 2, OC), BF16), vmem((TOK, OC), BF16), vmem((TOK, OC), BF16),
        dma((13,)), dma((2, 2, 20)), dma((2, 2, 20)), dma((7,)), dma((7,)), dma((15,)), dma((15,)),
        dma((9,)), dma((9,)), dma((9,)), dma((9,)), dma((4,)), dma((4,)), dma((2,)), dma((2,)),
        dma((4,)), dma((4,)),
    ]
    return pl.pallas_call(
        kernel,
        out_shape=jax.ShapeDtypeStruct((TOK, OC), BF16),
        in_specs=[any_spec] * 13,
        out_specs=any_spec,
        scratch_shapes=scratch,
        compiler_params=pltpu.CompilerParams(
            collective_id=0, has_side_effects=True, vmem_limit_bytes=66_000_000
        ),
        name="layer",
    )(
        residual, values, forget_onward, forget_reverse, surge_log_decay, gate_limit_complement,
        readout_query, output_gate, head_norm_gain.reshape(1, HD), output_weight,
        mixer_norm_gain.reshape(8, OC), up_weight, down_weight,
    )


def solution(mesh):
    both = P("sp", "tp")
    placed = (
        both, both, both, both, both, P(None, "tp"), both, both, P(), P("tp", None), P(), both, both,
    )
    return jax.shard_map(
        per_device, mesh=mesh, in_specs=placed, out_specs=both, check_vma=False
    )
```

time: 505 us -> 158 us (0.31)
  the two profiles are of different devices: /device:TPU:1 before, /device:TPU:17 now
where the time goes in v1:
time: 158 us; the launch traced here: 156 us
  Pallas kernels  151 us (96%)
  local copies, waits for them, and re-layouts  5.01 us (3%)
    pallas_call x1, Pallas kernels, per_device(): pl.pallas_call(kernel, out_shape=jax.ShapeDtypeStruct((TOK, OC), BF16), i...  151 us
    unnamed x2, local copies, waits for them, and re-layouts  3.69 us

profile of v1, /device:TPU:17, one launch (start us, length us, event | category | flops | bytes accessed | tf_op | source)
XLA Modules:
  0.0 156.1 jit_solution(8531469242830710681)
XLA Ops:
  0.0 1.3 reshape.7.norm_gain
  1.3 1.6 %copy.14.surge = f32[768,2]{1,0:T(8,128)} copy(f32[768,2]{0,1:T(2,128)} %param.17) | data formatting | bytes 12288 | tf_op args[4]
  2.9 151.1 %layer.1 = bf16[768,512]{1,0:T(8,128)(2,1)} custom-call(bf16[768,512]{1,0:T(8,128)(2,1)} %residual.1, bf16[768,256]{1,0:T(8,128)(2,1)} %values.1, bf16[768,256]{1,0:T(8,128)(2,1)} %f_on.1, bf16[768,256]{1,0:T(8,128)(2,1)} %f_rev.1, f32[768,2]{1,0:T(8,128)} %copy.14.surge, f32[2,256]{1,0:T(2,128)} %glc.1, bf16[768,256]{1,0:T(8,128)(2,1)} %query.1, ...), custom_call_target="tpu_custom_call" | custom-call | tf_op jit(solution)/shard_map/layer/pallas_call | solution.py:570
  154.1 2.1 %copy.16 = bf16[768,512]{1,0:T(8,128)(2,1)} copy(bf16[768,512]{1,0:T(8,128)(2,1)} %layer.1) | data formatting | bytes 1572864

commit v2 on v1

v2 whole, which is shorter than its diff:
```python
import functools

import jax
import jax.numpy as jnp
from jax import lax
from jax.experimental import pallas as pl
from jax.experimental.pallas import tpu as pltpu
from jax.sharding import PartitionSpec as P

D = 4096
HD = 128
HEADS = 2
CH = HEADS * HD
TOK = 768
BLK = 64
UNROLL = 3
NB = TOK // BLK
OC = 512
FFL = 1024
SHARD = 256
QUARTER = 64
EPS = 1e-06
MESH = pl.DeviceIdType.MESH
F32 = jnp.float32
BF16 = jnp.bfloat16
ST_ROWS = 272


def dot(a, b, dims=(((1,), (0,)), ((), ()))):
    return lax.dot_general(a, b, dims, preferred_element_type=F32)


LAST = (((1,), (1,)), ((), ()))
FIRST = (((0,), (0,)), ((), ()))


def sigmoid(x):
    return 1.0 / (1.0 + jnp.exp(-x))


def kernel(
    residual, values, f_on, f_rev, surge, glc, query, gate, head_gain, out_w,
    norm_gain, up_w, down_w,
    out,
    res_v, val_v, fon_v, frev_v, sur_t, sur_v, glc_v, que_v, gat_v, hg_v, ng_v,
    wu, wd, owc, ga, xa,
    qd, kr, sx, em, elx, run_state, run_log, row_in, col_in, sin, o_v, att,
    xg, ss, acc, hid,
    pp, d2r, ra, ee,
    in_sem, w_send, w_recv, ow_send, ow_recv, st_send, st_recv,
    g_send, g_recv, x_send, x_recv, c_send, c_recv, r_send, r_recv, e_send, e_recv,
):
    sp, tp = lax.axis_index("sp"), lax.axis_index("tp")
    x, z = lax.rem(sp, 4), lax.div(sp, 4)
    core, y = lax.rem(tp, 2), lax.div(tp, 2)
    other = 1 - core

    cur = [None]

    def mark(name):
        if cur[0] is not None:
            cur[0].__exit__(None, None, None)
        cur[0] = jax.named_scope(name) if name else None
        if name:
            cur[0].__enter__()

    mark("start")

    def ring(v, k):
        return lax.rem(v + (k % 4), 4)

    yp, ym, y2 = ring(y, 1), ring(y, 3), ring(y, 2)
    partner = 2 * y + other

    barrier = pltpu.get_barrier_semaphore()
    for o in range(1, 16):
        pl.semaphore_signal(barrier, inc=1, device_id=(lax.rem(sp + o, 16), tp), device_id_type=MESH)
    for o in range(1, 8):
        pl.semaphore_signal(barrier, inc=1, device_id=(sp, lax.rem(tp + o, 8)), device_id_type=MESH)

    own_rows = pl.ds(pl.multiple_of(sp * SHARD, SHARD), SHARD)
    ow_rows = pl.ds(pl.multiple_of(tp * 256, 256), 256)
    own_cols = pl.ds(pl.multiple_of(tp * OC, OC), OC)
    loads = [
        (f_on, fon_v), (f_rev, frev_v), (surge, sur_t.at[pl.ds(0, HEADS)]), (glc, glc_v), (query, que_v),
        (values, val_v), (gate, gat_v), (head_gain, hg_v), (residual, res_v), (norm_gain, ng_v),
        (up_w, wu.at[own_rows]), (down_w, wd.at[own_rows]),
        (out_w.at[:, own_cols], owc.at[ow_rows]),
    ]
    loads = [pltpu.make_async_copy(a, b, in_sem.at[i]) for i, (a, b) in enumerate(loads)]
    for copy in loads:
        copy.start()

    pl.semaphore_wait(barrier, 22)

    def remote(src, dst, ss_, rs_, dev):
        return pltpu.make_async_remote_copy(
            src_ref=src, dst_ref=dst, send_sem=ss_, recv_sem=rs_, device_id=dev, device_id_type=MESH
        )

    started = []

    def send(*args):
        copy = remote(*args)
        copy.start()
        started.append(copy)

    weights = ((up_w, wu), (down_w, wd))

    def sp_at(half, i, j):
        return ring(z, j) * 4 + ring(x, i) if half == 0 else ring(z, i) * 4 + ring(x, j)

    def piece(t, half, i, j, part):
        start, size = (0, 2 * QUARTER) if part is None else (part * QUARTER, QUARTER)
        first = sp_at(half, i, j) * SHARD + half * 2 * QUARTER + start
        return weights[t][1].at[pl.ds(pl.multiple_of(first, QUARTER), size)]

    FWD = (0, -1, 1, 2)

    def w_copy(t, half, slot, i, j, part, to, src=None):
        ref = piece(t, half, i, j, part)
        return remote(
            ref if src is None else src, ref, w_send.at[t, half, slot], w_recv.at[t, half, slot],
            (sp_at(half, *to), tp),
        )

    def w_go(*args, **kw):
        copy = w_copy(*args, **kw)
        copy.start()
        started.append(copy)

    def w_got(t, half, slot, i, j, part):
        w_copy(t, half, slot, i, j, part, (1, 0)).wait_recv()

    def w_second(t, half, n, src=None):
        i = FWD[n]
        w_go(t, half, 4 + 4 * n, i, 0, None, (0, 1), src=src)
        w_go(t, half, 5 + 4 * n, i, 0, None, (0, -1), src=src)

    def w_second_forward(t, half, n):
        i = FWD[n]
        w_got(t, half, 4 + 4 * n, i, -1, None)
        w_go(t, half, 6 + 4 * n, i, -1, 0, (0, 1))
        w_got(t, half, 5 + 4 * n, i, 1, None)
        w_go(t, half, 7 + 4 * n, i, 1, 1, (0, -1))

    def level0a(t):
        for half in range(2):
            src = weights[t][0].at[pl.ds(half * 2 * QUARTER, 2 * QUARTER)]
            w_go(t, half, 0, 0, 0, None, (1, 0), src=src)
            w_go(t, half, 1, 0, 0, None, (-1, 0), src=src)

    def level0b(t, half):
        src = weights[t][0].at[pl.ds(half * 2 * QUARTER, 2 * QUARTER)]
        w_second(t, half, 0, src=src)

    def level1a(t):
        for half in range(2):
            w_got(t, half, 0, -1, 0, None)
            w_go(t, half, 2, -1, 0, 0, (1, 0))
            w_got(t, half, 1, 1, 0, None)
            w_go(t, half, 3, 1, 0, 1, (-1, 0))
        for half in range(2):
            w_second(t, half, 1)
            w_second(t, half, 2)

    def level1b(t):
        for half in range(2):
            w_second_forward(t, half, 0)

    def level2(t):
        for half in range(2):
            w_got(t, half, 2, 2, 0, 0)
            w_got(t, half, 3, 2, 0, 1)
            w_second(t, half, 3)
        for half in range(2):
            w_second_forward(t, half, 1)
            w_second_forward(t, half, 2)

    def level3(t):
        for half in range(2):
            w_second_forward(t, half, 3)

    def level4(t, blocks=(0, 1, 2, 3)):
        for half in range(2):
            for n in blocks:
                w_got(t, half, 6 + 4 * n, FWD[n], 2, 0)
                w_got(t, half, 7 + 4 * n, FWD[n], 2, 1)

    mark("w0")
    level0a(0)

    def ow_copy(o):
        to = lax.rem(tp + o, 8)
        return remote(
            out_w.at[:, pl.ds(pl.multiple_of(to * OC, OC), OC)], owc.at[ow_rows],
            ow_send.at[o - 1], ow_recv.at[o - 1], (sp, to),
        )

    for o in range(1, 8):
        copy = ow_copy(o)
        copy.start()
        started.append(copy)

    mark("loadwait")
    for copy in loads[:7]:
        copy.wait()

    mark("pass1")
    row_id = lax.broadcasted_iota(jnp.int32, (BLK, BLK), 0)
    col_id = lax.broadcasted_iota(jnp.int32, (BLK, BLK), 1)
    lower, upper = row_id >= col_id, row_id <= col_id
    run_state[...] = jnp.zeros_like(run_state)
    run_log[...] = jnp.zeros_like(run_log)
    sur_v[...] = jnp.concatenate([sur_t[0:HEADS, :], jnp.zeros((8 - HEADS, TOK), F32)], axis=0).T
    sums = tuple(
        jnp.concatenate([jnp.where(tri, 1.0, 0.0)] * 3, axis=1).astype(BF16) for tri in (lower, upper)
    )

    def split3(v):
        a = v.astype(BF16)
        rest = v - a.astype(F32)
        b = rest.astype(BF16)
        return jnp.concatenate([a, b, (rest - b.astype(F32)).astype(BF16)], axis=0)

    def pass1_block(d, blk):
        logits = (fon_v, frev_v)[d]
        mid_at, end_at = ((BLK // 2 - 1, BLK - 1), (BLK // 2, 0))[d]
        rows = pl.ds(pl.multiple_of(blk * BLK, BLK), BLK)
        key = glc_v[d : d + 1, :] / (1.0 + jnp.exp(logits[rows, :].astype(F32)))
        sg = sur_v[rows, :]
        sg = jnp.concatenate(
            [jnp.broadcast_to(sg[:, h : h + 1], (BLK, HD)) for h in range(HEADS)], axis=1
        )
        run = dot(sums[d], split3(jnp.log1p(-key) + sg))
        mid, end = run[mid_at : mid_at + 1, :], run[end_at : end_at + 1, :]
        q = que_v[rows, :].astype(F32)
        q = q * sigmoid(q) * (HD ** -0.5)
        qd[d, rows, :] = (q * jnp.exp(run - mid)).astype(BF16)
        k = key * jnp.exp(mid - run)
        kr[d, rows, :] = k.astype(BF16)
        tail = (k * jnp.exp(end - mid)).astype(BF16)
        v = val_v[rows, :]
        new = [
            dot(v[:, h * HD : (h + 1) * HD], tail[:, h * HD : (h + 1) * HD], FIRST)
            for h in range(HEADS)
        ]
        em[d, blk] = jnp.broadcast_to(jnp.exp(mid), (8, CH))
        return end, new

    def pass1(step, carry):
        blocks = [
            (d, step * UNROLL + u if d == 0 else NB - 1 - (step * UNROLL + u))
            for u in range(UNROLL)
            for d in range(2)
        ]
        parts = [pass1_block(d, blk) for d, blk in blocks]
        for (d, blk), (end, new) in zip(blocks, parts):
            gone = run_log[d, 0:1, :]
            elx[d, blk] = jnp.broadcast_to(jnp.exp(gone), (8, CH))
            run_log[d] = jnp.broadcast_to(gone + end, (8, CH))
            decay = jnp.exp(end)
            for h in range(HEADS):
                hs = slice(h * HD, (h + 1) * HD)
                state = run_state[d, hs, :]
                sx[d, blk, hs, :] = state.astype(BF16)
                run_state[d, hs, :] = state * decay[:, hs] + new[h]
        return carry

    lax.fori_loop(0, NB // UNROLL, pass1, 0)

    mark("stsend")
    def store_state(ref, at, d, state, log):
        ref[at, d, 0:CH, :] = state.astype(BF16)
        high = log.astype(BF16).astype(F32)
        rest = log - high
        ref[at, d, CH:ST_ROWS, :] = jnp.concatenate(
            [high[:, :HD], high[:, HD:], rest[:, :HD], rest[:, HD:], jnp.zeros((12, HD), F32)], axis=0
        ).astype(BF16)

    def load_log(ref, at, d):
        tail = ref[at, d, CH:ST_ROWS, :].astype(F32)
        return [tail[h : h + 1, :] + tail[2 + h : 3 + h, :] for h in range(HEADS)]

    for d in range(2):
        store_state(row_in, x, d, run_state[d], run_log[d, 0:1, :])

    def row_copy(o):
        return remote(
            row_in.at[x], row_in.at[x], st_send.at[o - 1], st_recv.at[o - 1],
            (z * 4 + ring(x, o), tp),
        )

    def row_got(o):
        ref = row_in.at[ring(x, -o)]
        remote(ref, ref, st_send.at[o - 1], st_recv.at[o - 1], (z * 4 + ring(x, o), tp)).wait_recv()

    def col_copy(o):
        ref = col_in.at[z, lax.div(z + o, 4)]
        return remote(
            ref, ref, st_send.at[o + 2], st_recv.at[o + 2], (ring(z, o) * 4 + x, tp)
        )

    def col_got(o):
        ref = col_in.at[ring(z, -o), lax.div(z + 4 - o, 4) * -1 + 1]
        remote(ref, ref, st_send.at[o + 2], st_recv.at[o + 2], (ring(z, o) * 4 + x, tp)).wait_recv()

    for o in (1, 3, 2):
        copy = row_copy(o)
        copy.start()
        started.append(copy)
    mark("l0b")
    level0b(0, 0)

    def pass2_block(blk):
        rows = pl.ds(pl.multiple_of(blk * BLK, BLK), BLK)
        v = val_v[rows, :]
        for h in range(HEADS):
            hs = slice(h * HD, (h + 1) * HD)
            fwd = dot(qd[0, rows, hs], kr[0, rows, hs], LAST)
            bwd = dot(qd[1, rows, hs], kr[1, rows, hs], LAST)
            score = jnp.where(lower, fwd, 0.0) + jnp.where(upper, bwd, 0.0)
            o_v[rows, hs] = dot(score.astype(BF16), v[:, hs])

    def by_blocks(body):
        def step(i, carry):
            for u in range(UNROLL):
                body(i * UNROLL + u)
            return carry

        lax.fori_loop(0, NB // UNROLL, step, 0)

    mark("pass2")
    by_blocks(pass2_block)


    mark("roww")
    for o in (1, 3, 2):
        row_got(o)
    mark("rowc")
    for d in range(2):
        state = jnp.zeros((CH, HD), F32)
        log = [jnp.zeros((1, HD), F32)] * HEADS
        for j in range(4) if d == 0 else range(3, -1, -1):
            own = load_log(row_in, j, d)
            state = jnp.concatenate(
                [
                    state[h * HD : (h + 1) * HD] * jnp.exp(own[h])
                    + row_in[j, d, h * HD : (h + 1) * HD, :].astype(F32)
                    for h in range(HEADS)
                ],
                axis=0,
            )
            log = [log[h] + own[h] for h in range(HEADS)]
        store_state(col_in, z, d, state, jnp.concatenate(log, axis=1))
    for o in (1, 3, 2):
        copy = col_copy(o)
        copy.start()
        started.append(copy)
    level0b(0, 1)
    sin[...] = jnp.zeros_like(sin)
    mark("colw")
    for o in (1, 3, 2):
        col_got(o)
    level1a(0)
    mark("combine")

    def chain(ref, at):
        def body(i, carry):
            d = lax.div(i + 4 - at, 4)
            j = (1 - d) * i + d * (3 + at - i)
            own = load_log(ref, j, d)
            for h in range(HEADS):
                hs = slice(h * HD, (h + 1) * HD)
                sin[d, hs, :] = sin[d, hs, :] * jnp.exp(own[h]) + ref[j, d, hs, :].astype(F32)
            return carry

        lax.fori_loop(0, 3, body, 0)

    chain(col_in, z)
    chain(row_in, x)

    for copy in loads[6:10]:
        if copy is not loads[6]:
            copy.wait()

    def pass3_block(blk):
        rows = pl.ds(pl.multiple_of(blk * BLK, BLK), BLK)
        for h in range(HEADS):
            hs = slice(h * HD, (h + 1) * HD)
            mixed = o_v[rows, hs]
            for d in range(2):
                qs = (qd[d, rows, hs].astype(F32) * em[d, blk, 0:1, hs]).astype(BF16)
                state = sx[d, blk, hs, :].astype(F32) + elx[d, blk, 0:1, hs] * sin[d, hs, :]
                mixed = mixed + dot(qs, state.astype(BF16), LAST)
            norm = mixed * lax.rsqrt(jnp.mean(mixed * mixed, axis=-1, keepdims=True) + EPS)
            g = gat_v[rows, hs].astype(F32)
            ga[tp, rows, hs] = (norm * hg_v[0:1, :] * (g * sigmoid(g))).astype(BF16)

    mark("pass3")
    by_blocks(pass3_block)

    HALF = TOK // 2

    class Gather:
        def __init__(self, buf, send_sem, recv_sem):
            self.buf, self.ss, self.rs = buf, send_sem, recv_sem

        def copy(self, k, slot, part, to):
            ref = self.buf.at[slot]
            if part is not None:
                ref = self.buf.at[slot, pl.ds(part * HALF, HALF)]
            return remote(ref, ref, self.ss.at[k], self.rs.at[k], (sp, to))

        def go(self, *args):
            copy = self.copy(*args)
            copy.start()
            started.append(copy)

        def got(self, k, slot, part):
            self.copy(k, slot, part, partner).wait_recv()

        def own(self):
            self.go(0, tp, None, 2 * yp + core)
            self.go(1, tp, None, 2 * ym + core)
            self.go(4, tp, None, partner)

        def from_side(self):
            left, right = 2 * ym + core, 2 * yp + core
            self.got(0, left, None)
            self.go(2, left, 0, right)
            self.go(5, left, None, partner)
            self.got(1, right, None)
            self.go(3, right, 1, left)
            self.go(6, right, None, partner)

        def from_far(self):
            far = 2 * y2 + core
            self.got(2, far, 0)
            self.go(7, far, 0, partner)
            self.got(3, far, 1)
            self.go(8, far, 1, partner)

    gathered = Gather(ga, g_send, g_recv)
    mark("gown")
    gathered.own()

    mark("owwait")
    for copy in loads[10:13]:
        copy.wait()
    for o in range(1, 8):
        ow_copy(o).wait_recv()

    def project(block, first=False):
        def tile(n, carry):
            cols = pl.ds(pl.multiple_of(n * 256, 256), 256)
            part = dot(ga[block], owc[pl.ds(pl.multiple_of(block * 256, 256), 256), cols])
            att[:, cols] = part if first else att[:, cols] + part
            return carry

        lax.fori_loop(0, OC // 256, tile, 0)

    mark("proj0")
    project(tp, True)
    mark("gpart")
    gathered.got(4, partner, None)
    project(partner)
    mark("gside")
    gathered.from_side()
    mark("proj2")
    project(2 * ym + core)
    project(2 * yp + core)
    mark("lev1b_0")
    level1b(0)
    mark("gpart2")
    gathered.got(5, 2 * ym + other, None)
    project(2 * ym + other)
    gathered.got(6, 2 * yp + other, None)
    project(2 * yp + other)
    mark("gfar")
    gathered.from_far()
    project(2 * y2 + core)
    gathered.got(7, 2 * y2 + other, 0)
    gathered.got(8, 2 * y2 + other, 1)
    project(2 * y2 + other)

    TILE = 128

    def middle(i, carry):
        rows = pl.ds(pl.multiple_of(i * TILE, TILE), TILE)
        xa[tp, rows, :] = (res_v[rows, :].astype(F32) + att[rows, :]).astype(BF16)
        return carry

    mark("middle")
    lax.fori_loop(0, TOK // TILE, middle, 0)

    spread = Gather(xa, x_send, x_recv)
    spread.own()
    def scale(chip, c, first=False):
        block = 2 * chip + c
        gain = ng_v[:, pl.ds(pl.multiple_of(block * OC, OC), OC)]
        cols = pl.ds(pl.multiple_of(c * OC, OC), OC)

        def body(i, carry):
            rows = pl.ds(pl.multiple_of(i * TILE, TILE), TILE)
            v = xa[block, rows, :].astype(F32)
            sq = v * v
            sq = (sq[:, 0:128] + sq[:, 128:256]) + (sq[:, 256:384] + sq[:, 384:512])
            ss[rows, :] = sq if first else ss[rows, :] + sq
            xg[rows, cols] = (v * gain).astype(BF16)
            return carry

        lax.fori_loop(0, TOK // TILE, body, 0)

    def lift(chip, first=False):
        def tile(n, carry):
            cols = pl.ds(pl.multiple_of(n * 256, 256), 256)
            part = dot(xg[...], wu[pl.ds(pl.multiple_of(chip * 2 * OC, 2 * OC), 2 * OC), cols])
            acc[:, cols] = part if first else acc[:, cols] + part
            return carry

        lax.fori_loop(0, FFL // 256, tile, 0)

    mark("lev2_0")
    level2(0)
    mark("scale0")
    scale(y, core, True)
    spread.got(4, partner, None)
    scale(y, other)
    mark("lev3_0")
    level3(0)
    level0a(1)
    level0b(1, 0)
    level0b(1, 1)
    mark("xside")
    spread.from_side()
    mark("lev4_0")
    level4(0)
    mark("lift0")
    lift(y, True)
    mark("lift1")
    scale(ym, core)
    spread.got(5, 2 * ym + other, None)
    scale(ym, other)
    lift(ym)
    mark("lev1_1")
    level1a(1)
    level1b(1)
    mark("lift2")
    scale(yp, core)
    spread.got(6, 2 * yp + other, None)
    scale(yp, other)
    lift(yp)
    mark("xfar")
    spread.from_far()
    mark("lift3")
    scale(y2, core)
    spread.got(7, 2 * y2 + other, 0)
    spread.got(8, 2 * y2 + other, 1)
    scale(y2, other)
    lift(y2)

    def activate(i, carry):
        rows = pl.ds(pl.multiple_of(i * TILE, TILE), TILE)
        total = jnp.sum(ss[rows, :], axis=-1, keepdims=True)
        v = jnp.maximum(acc[rows, :] * lax.rsqrt(total / D + EPS), 0.0)
        hid[rows, :] = (v * v).astype(BF16)
        return carry

    mark("act")
    lax.fori_loop(0, TOK // TILE, activate, 0)


    PAIRS = ((1, 0), (0, 0), (1, 1), (1, -1), (1, 2), (0, 1), (0, -1), (0, 2))

    class Step:
        def __init__(self, n):
            self.n = n
            self.dx, dz = PAIRS[n]
            zs = ring(z, dz)
            column = lax.rem(x + self.dx, 2)
            self.slot = self.dx * 4 + zs
            self.first = zs * 4 + column
            self.delta = lax.rem(zs + 4 - y, 4)
            self.odd = lax.rem(self.delta, 2) == 1
            self.far = self.delta == 2
            self.k = lax.div(self.delta, 2)
            self.to = 2 * lax.rem(y + self.delta, 4) + core

        def chip(self):
            return remote(
                pp.at[0, self.slot], d2r.at[self.slot], c_send.at[self.n], c_recv.at[self.n], (sp, partner)
            )

        def half(self, k):
            return pl.ds(pl.multiple_of(k * HALF, HALF), HALF)

        def out_far(self, k):
            return remote(
                pp.at[1, self.slot, self.half(k)], ra.at[self.slot], r_send.at[self.n, k],
                r_recv.at[self.n], (sp, 2 * (yp, ym)[k] + core),
            )

        def out_near(self, k):
            return remote(
                pp.at[1, self.slot, self.half(k)], ee.at[self.k, self.dx, self.half(k)],
                e_send.at[self.n, k], e_recv.at[self.k, self.dx, k], (sp, self.to),
            )

        def compute(self):
            mark("comp%d" % self.n)
            def part(i, carry):
                first = (self.first + 2 * (other + i * (core - other))) * SHARD
                rows = wd[pl.ds(pl.multiple_of(first, SHARD), SHARD), :]
                pp[i, self.slot] = dot(hid[...], rows, LAST).astype(BF16)

                @pl.when(i == 0)
                def _():
                    self.chip().start()

                return carry

            lax.fori_loop(0, 2, part, 0)
            started.append(self.chip())

        def chip_sum(self):
            mark("cs%d" % self.n)
            self.chip().wait_recv()

            def add(i, carry):
                rows = pl.ds(pl.multiple_of(i * TILE, TILE), TILE)
                total = pp[1, self.slot, rows, :].astype(F32) + d2r[self.slot, rows, :].astype(F32)
                pp[1, self.slot, rows, :] = total.astype(BF16)
                return carry

            lax.fori_loop(0, TOK // TILE, add, 0)

            @pl.when(self.far)
            def _():
                self.out_far(0).start()
                self.out_far(1).start()

            @pl.when(self.odd)
            def _():
                self.out_near(1 - self.k).start()

        def join(self):
            mark("jn%d" % self.n)
            @pl.when(self.odd)
            def _():
                remote(
                    ra.at[self.slot], ra.at[self.slot], r_send.at[self.n, 0], r_recv.at[self.n],
                    (sp, self.to),
                ).wait_recv()

                def add(i, carry):
                    rows = pl.ds(pl.multiple_of(self.k * HALF + i * TILE, TILE), TILE)
                    got = ra[self.slot, pl.ds(pl.multiple_of(i * TILE, TILE), TILE), :]
                    total = pp[1, self.slot, rows, :].astype(F32) + got.astype(F32)
                    pp[1, self.slot, rows, :] = total.astype(BF16)
                    return carry

                lax.fori_loop(0, HALF // TILE, add, 0)
                self.out_near(self.k).start()

        def drain(self):
            @pl.when(self.far)
            def _():
                self.out_far(0).wait_send()
                self.out_far(1).wait_send()

            @pl.when(self.odd)
            def _():
                self.out_near(1 - self.k).wait_send()
                self.out_near(self.k).wait_send()

    steps = [Step(n) for n in range(8)]
    steps[0].compute()
    mark("lev2_1")
    level2(1)
    level4(1, (0,))
    steps[1].compute()
    steps[0].chip_sum()
    steps[2].compute()
    steps[1].chip_sum()
    steps[3].compute()
    steps[2].chip_sum()
    steps[0].join()
    mark("lev3_1")
    level3(1)
    level4(1, (1, 2))
    steps[4].compute()
    steps[3].chip_sum()
    steps[1].join()
    steps[5].compute()
    steps[4].chip_sum()
    steps[2].join()
    steps[6].compute()
    steps[5].chip_sum()
    steps[3].join()
    mark("lev4_1")
    level4(1, (3,))
    steps[7].compute()
    steps[6].chip_sum()
    mark("d8")
    steps[7].chip_sum()
    for n in range(4, 8):
        mark("j%d" % n)
        steps[n].join()
    mark("ewait")

    for dx in range(2):
        slot = dx * 4 + y
        for k in range(2):
            for half in range(2):
                rows = pl.ds(half * HALF, HALF)
                remote(
                    ee.at[k, dx, rows], ee.at[k, dx, rows], e_send.at[0, 0], e_recv.at[k, dx, half],
                    (sp, partner),
                ).wait_recv()
        cols = pl.ds(pl.multiple_of(lax.rem(x + dx, 2) * SHARD, SHARD), SHARD)

        def finish(i, carry):
            rows = pl.ds(pl.multiple_of(i * TILE, TILE), TILE)
            total = pp[1, slot, rows, :].astype(F32)
            total = total + (ee[0, dx, rows, :].astype(F32) + ee[1, dx, rows, :].astype(F32))
            res_v[rows, cols] = (xa[tp, rows, cols].astype(F32) + total).astype(BF16)
            return carry

        lax.fori_loop(0, TOK // TILE, finish, 0)
    mark("final")
    final = pltpu.make_async_copy(res_v, out, in_sem.at[0])
    final.start()
    for copy in started:
        copy.wait_send()
    for step in steps:
        step.drain()
    final.wait()
    mark(None)


def per_device(
    residual, values, forget_onward, forget_reverse, surge_log_decay, gate_limit_complement,
    readout_query, output_gate, head_norm_gain, output_weight, mixer_norm_gain, up_weight,
    down_weight,
):
    any_spec = pl.BlockSpec(memory_space=pl.ANY)
    vmem, dma = pltpu.VMEM, pltpu.SemaphoreType.DMA
    scratch = [
        vmem((TOK, OC), BF16), vmem((TOK, CH), BF16), vmem((TOK, CH), BF16), vmem((TOK, CH), BF16),
        vmem((8, TOK), F32), vmem((TOK, 8), F32), vmem((2, CH), F32), vmem((TOK, CH), BF16), vmem((TOK, CH), BF16),
        vmem((1, HD), F32), vmem((1, D), F32),
        vmem((D, FFL), BF16), vmem((D, FFL), BF16), vmem((2048, OC), BF16),
        vmem((8, TOK, CH), BF16), vmem((8, TOK, OC), BF16),
        vmem((2, TOK, CH), BF16), vmem((2, TOK, CH), BF16), vmem((2, NB, CH, HD), BF16),
        vmem((2, NB, 8, CH), F32), vmem((2, NB, 8, CH), F32),
        vmem((2, CH, HD), F32), vmem((2, 8, CH), F32),
        vmem((4, 2, ST_ROWS, HD), BF16), vmem((4, 2, ST_ROWS, HD), BF16), vmem((2, CH, HD), F32),
        vmem((TOK, CH), F32), vmem((TOK, OC), F32),
        vmem((TOK, 2 * OC), BF16), vmem((TOK, HD), F32), vmem((TOK, FFL), F32), vmem((TOK, FFL), BF16),
        vmem((2, 8, TOK, SHARD), BF16), vmem((8, TOK, SHARD), BF16),
        vmem((8, TOK // 2, SHARD), BF16), vmem((2, 2, TOK, SHARD), BF16),
        dma((13,)), dma((2, 2, 20)), dma((2, 2, 20)), dma((7,)), dma((7,)), dma((6,)), dma((6,)),
        dma((9,)), dma((9,)), dma((9,)), dma((9,)), dma((8,)), dma((8,)), dma((8, 2)), dma((8,)),
        dma((8, 2)), dma((2, 2, 2)),
    ]
    return pl.pallas_call(
        kernel,
        out_shape=jax.ShapeDtypeStruct((TOK, OC), BF16),
        in_specs=[any_spec] * 13,
        out_specs=any_spec,
        scratch_shapes=scratch,
        compiler_params=pltpu.CompilerParams(
            collective_id=0, has_side_effects=True, vmem_limit_bytes=66_000_000
        ),
        name="layer",
    )(
        residual, values, forget_onward, forget_reverse, surge_log_decay.T, gate_limit_complement,
        readout_query, output_gate, head_norm_gain.reshape(1, HD), output_weight,
        mixer_norm_gain.reshape(1, D), up_weight, down_weight,
    )


def solution(mesh):
    both = P("sp", "tp")
    placed = (
        both, both, both, both, both, P(None, "tp"), both, both, P(), P("tp", None), P(), both, both,
    )
    return jax.shard_map(
        per_device, mesh=mesh, in_specs=placed, out_specs=both, check_vma=False
    )
```

time: 158 us -> 141 us (0.89)
  Pallas kernels: 151 us -> 137 us
  local copies, waits for them, and re-layouts: 5.01 us -> 2.06 us
    pallas_call x1, Pallas kernels: 151 us -> 137 us  [per_device(): pl.pallas_call(kernel, out_shape=jax.ShapeDtypeStruct((TOK, OC), BF16), i...]
    unnamed x2 -> x1, local copies, waits for them, and re-layouts: 3.69 us -> 2.06 us
where the time goes in v2:
time: 141 us; the launch traced here: 139 us
  Pallas kernels  137 us (97%)
  local copies, waits for them, and re-layouts  2.06 us (1%)
    pallas_call x1, Pallas kernels, per_device(): pl.pallas_call(kernel, out_shape=jax.ShapeDtypeStruct((TOK, OC), BF16), i...  137 us

profile of v2, /device:TPU:17, one launch (start us, length us, event | category | flops | bytes accessed | tf_op | source)
XLA Modules:
  0.0 139.5 jit_solution(7031701284007788404)
XLA Ops:
  0.0 137.4 %layer.1 = bf16[768,512]{1,0:T(8,128)(2,1)} custom-call(bf16[768,512]{1,0:T(8,128)(2,1)} %residual.1, bf16[768,256]{1,0:T(8,128)(2,1)} %values.1, bf16[768,256]{1,0:T(8,128)(2,1)} %f_on.1, bf16[768,256]{1,0:T(8,128)(2,1)} %f_rev.1, f32[2,768]{1,0:T(2,128)} %bitcast.4, f32[2,256]{1,0:T(2,128)} %glc.1, bf16[768,256]{1,0:T(8,128)(2,1)} %query.1, ...), custom_call_target="tpu_custom_call" | custom-call | tf_op jit(solution)/shard_map/layer/pallas_call | solution.py:767
  137.4 2.1 %copy.15 = bf16[768,512]{1,0:T(8,128)(2,1)} copy(bf16[768,512]{1,0:T(8,128)(2,1)} %layer.1) | data formatting | bytes 1572864

commit v3 on v2

--- a/solution.py
+++ b/solution.py
@@ -46,7 +46,7 @@
     wu, wd, owc, ga, xa,
     qd, kr, sx, em, elx, run_state, run_log, row_in, col_in, sin, o_v, att,
     xg, ss, acc, hid,
-    pp, d2r, ra, ee,
+    pp, d2r, ra, ee, relay,
     in_sem, w_send, w_recv, ow_send, ow_recv, st_send, st_recv,
     g_send, g_recv, x_send, x_recv, c_send, c_recv, r_send, r_recv, e_send, e_recv,
 ):
@@ -100,8 +100,7 @@
 
     started = []
 
-    def send(*args):
-        copy = remote(*args)
+    def go(copy):
         copy.start()
         started.append(copy)
 
@@ -168,39 +167,84 @@
         for half in range(2):
             w_second_forward(t, half, 0)
 
-    def level2(t):
-        for half in range(2):
-            w_got(t, half, 2, 2, 0, 0)
-            w_got(t, half, 3, 2, 0, 1)
-            w_second(t, half, 3)
-        for half in range(2):
-            w_second_forward(t, half, 1)
-            w_second_forward(t, half, 2)
-
-    def level3(t):
-        for half in range(2):
-            w_second_forward(t, half, 3)
-
-    def level4(t, blocks=(0, 1, 2, 3)):
-        for half in range(2):
-            for n in blocks:
-                w_got(t, half, 6 + 4 * n, FWD[n], 2, 0)
-                w_got(t, half, 7 + 4 * n, FWD[n], 2, 1)
+    def level2a(t, half):
+        w_got(t, half, 2, 2, 0, 0)
+        w_got(t, half, 3, 2, 0, 1)
+        w_second(t, half, 3)
+
+    def level2b(t, half):
+        w_second_forward(t, half, 1)
+        w_second_forward(t, half, 2)
+
+    def level3(t, half):
+        w_second_forward(t, half, 3)
+
+    def level4(t, half, blocks):
+        for n in blocks:
+            w_got(t, half, 6 + 4 * n, FWD[n], 2, 0)
+            w_got(t, half, 7 + 4 * n, FWD[n], 2, 1)
 
     mark("w0")
     level0a(0)
 
-    def ow_copy(o):
-        to = lax.rem(tp + o, 8)
+    def ow_cols(to):
+        return pl.ds(pl.multiple_of(to * OC, OC), OC)
+
+    def ow_rows_of(source, k=None):
+        first, size = (0, 256) if k is None else (k * 128, 128)
+        return pl.ds(pl.multiple_of(source * 256 + first, 128), size)
+
+    near = (yp, ym)
+
+    def ow_leg1(k, c):
         return remote(
-            out_w.at[:, pl.ds(pl.multiple_of(to * OC, OC), OC)], owc.at[ow_rows],
-            ow_send.at[o - 1], ow_recv.at[o - 1], (sp, to),
+            out_w.at[pl.ds(k * 128, 128), ow_cols(2 * y2 + c)], relay.at[k, c],
+            ow_send.at[2 * k + c], ow_recv.at[2 * k + c], (sp, 2 * near[k] + core),
         )
 
-    for o in range(1, 8):
-        copy = ow_copy(o)
-        copy.start()
-        started.append(copy)
+    def ow_direct(k, c):
+        return remote(
+            out_w.at[:, ow_cols(2 * near[k] + c)], owc.at[ow_rows],
+            ow_send.at[4 + 2 * k + c], ow_recv.at[4 + 2 * k + core], (sp, 2 * near[k] + c),
+        )
+
+    def ow_partner():
+        return remote(
+            out_w.at[:, ow_cols(partner)], owc.at[ow_rows], ow_send.at[8], ow_recv.at[8], (sp, partner)
+        )
+
+    def ow_leg2(k, c):
+        return remote(
+            relay.at[k, c], owc.at[ow_rows_of(2 * near[1 - k] + core, k)],
+            ow_send.at[9 + 2 * k + c], ow_recv.at[9 + 2 * k + core], (sp, 2 * near[k] + c),
+        )
+
+    def ow_forward():
+        for k in range(2):
+            for c in range(2):
+                ow_leg1(k, c).wait_recv()
+                go(ow_leg2(k, c))
+
+    def ow_wait():
+        def landed(rows, sem):
+            ref = owc.at[rows]
+            remote(ref, ref, ow_send.at[8], ow_recv.at[sem], (sp, partner)).wait_recv()
+
+        landed(ow_rows_of(partner), 8)
+        for k in range(2):
+            for c in range(2):
+                landed(ow_rows_of(2 * near[1 - k] + c), 4 + 2 * k + c)
+        for k in range(2):
+            for c in range(2):
+                landed(ow_rows_of(2 * y2 + c, k), 9 + 2 * k + c)
+
+    for k in range(2):
+        for c in range(2):
+            go(ow_leg1(k, c))
+    for k in range(2):
+        for c in range(2):
+            go(ow_direct(k, c))
+    go(ow_partner())
 
     mark("loadwait")
     for copy in loads[:7]:
@@ -334,6 +378,8 @@
     by_blocks(pass2_block)
 
 
+    mark("owfwd")
+    ow_forward()
     mark("roww")
     for o in (1, 3, 2):
         row_got(o)
@@ -421,25 +467,33 @@
             self.copy(k, slot, part, partner).wait_recv()
 
         def own(self):
-            self.go(0, tp, None, 2 * yp + core)
-            self.go(1, tp, None, 2 * ym + core)
-            self.go(4, tp, None, partner)
+            right, left = 2 * yp + core, 2 * ym + core
+            self.go(0, tp, 0, right)
+            self.go(3, tp, 1, left)
+            self.go(6, tp, None, partner)
+            self.go(1, tp, 1, right)
+            self.go(2, tp, 0, left)
+
+        def forward(self):
+            left, right = 2 * ym + core, 2 * yp + core
+            self.got(0, left, 0)
+            self.go(4, left, 0, right)
+            self.got(3, right, 1)
+            self.go(5, right, 1, left)
 
         def from_side(self):
             left, right = 2 * ym + core, 2 * yp + core
-            self.got(0, left, None)
-            self.go(2, left, 0, right)
-            self.go(5, left, None, partner)
-            self.got(1, right, None)
-            self.go(3, right, 1, left)
-            self.go(6, right, None, partner)
+            self.got(1, left, 1)
+            self.go(7, left, None, partner)
+            self.got(2, right, 0)
+            self.go(8, right, None, partner)
 
         def from_far(self):
             far = 2 * y2 + core
-            self.got(2, far, 0)
-            self.go(7, far, 0, partner)
-            self.got(3, far, 1)
-            self.go(8, far, 1, partner)
+            self.got(4, far, 0)
+            self.go(9, far, 0, partner)
+            self.got(5, far, 1)
+            self.go(10, far, 1, partner)
 
     gathered = Gather(ga, g_send, g_recv)
     mark("gown")
@@ -448,8 +502,7 @@
     mark("owwait")
     for copy in loads[10:13]:
         copy.wait()
-    for o in range(1, 8):
-        ow_copy(o).wait_recv()
+    ow_wait()
 
     def project(block, first=False):
         def tile(n, carry):
@@ -463,25 +516,33 @@
     mark("proj0")
     project(tp, True)
     mark("gpart")
-    gathered.got(4, partner, None)
+    gathered.got(6, partner, None)
     project(partner)
+    mark("lev2a_0")
+    level1b(0)
+    level2a(0, 0)
+    level2a(0, 1)
+    mark("gfwd")
+    gathered.forward()
     mark("gside")
     gathered.from_side()
     mark("proj2")
     project(2 * ym + core)
     project(2 * yp + core)
-    mark("lev1b_0")
-    level1b(0)
+    mark("lev2b_0")
+    level2b(0, 0)
+    level2b(0, 1)
+    level0a(1)
     mark("gpart2")
-    gathered.got(5, 2 * ym + other, None)
+    gathered.got(7, 2 * ym + other, None)
     project(2 * ym + other)
-    gathered.got(6, 2 * yp + other, None)
+    gathered.got(8, 2 * yp + other, None)
     project(2 * yp + other)
     mark("gfar")
     gathered.from_far()
     project(2 * y2 + core)
-    gathered.got(7, 2 * y2 + other, 0)
-    gathered.got(8, 2 * y2 + other, 1)
+    gathered.got(9, 2 * y2 + other, 0)
+    gathered.got(10, 2 * y2 + other, 1)
     project(2 * y2 + other)
 
     TILE = 128
@@ -521,42 +582,45 @@
 
         lax.fori_loop(0, FFL // 256, tile, 0)
 
-    mark("lev2_0")
-    level2(0)
     mark("scale0")
     scale(y, core, True)
-    spread.got(4, partner, None)
+    spread.got(6, partner, None)
     scale(y, other)
     mark("lev3_0")
-    level3(0)
-    level0a(1)
+    level3(0, 0)
+    level3(0, 1)
     level0b(1, 0)
     level0b(1, 1)
+    mark("xfwd")
+    spread.forward()
+    mark("lev1a_1")
+    level1a(1)
     mark("xside")
     spread.from_side()
     mark("lev4_0")
-    level4(0)
+    level4(0, 0, range(4))
+    level4(0, 1, range(4))
     mark("lift0")
     lift(y, True)
     mark("lift1")
     scale(ym, core)
-    spread.got(5, 2 * ym + other, None)
+    spread.got(7, 2 * ym + other, None)
     scale(ym, other)
     lift(ym)
     mark("lev1_1")
-    level1a(1)
     level1b(1)
+    level2a(1, 1)
     mark("lift2")
     scale(yp, core)
-    spread.got(6, 2 * yp + other, None)
+    spread.got(8, 2 * yp + other, None)
     scale(yp, other)
     lift(yp)
     mark("xfar")
     spread.from_far()
     mark("lift3")
     scale(y2, core)
-    spread.got(7, 2 * y2 + other, 0)
-    spread.got(8, 2 * y2 + other, 1)
+    spread.got(9, 2 * y2 + other, 0)
+    spread.got(10, 2 * y2 + other, 1)
     scale(y2, other)
     lift(y2)
 
@@ -571,14 +635,20 @@
     lax.fori_loop(0, TOK // TILE, activate, 0)
 
 
-    PAIRS = ((1, 0), (0, 0), (1, 1), (1, -1), (1, 2), (0, 1), (0, -1), (0, 2))
+    SHARDS = (
+        (1, 0), (0, 0), (1, 1), (1, -1), (1, 2), (0, 1), (0, -1), (0, 2), (2, 2)
+    )
 
     class Step:
         def __init__(self, n):
             self.n = n
-            self.dx, dz = PAIRS[n]
+            dx, dz = SHARDS[n]
+            self.single = n >= 7
+            self.dx = dx % 2
             zs = ring(z, dz)
-            column = lax.rem(x + self.dx, 2)
+            column = lax.rem(x + dx, 2)
+            self.keep = lax.div(ring(x, dx), 2) == core
+            self.kept = jnp.where(self.keep, 1, 0)
             self.slot = self.dx * 4 + zs
             self.first = zs * 4 + column
             self.delta = lax.rem(zs + 4 - y, 4)
@@ -620,11 +690,22 @@
 
                 return carry
 
-            lax.fori_loop(0, 2, part, 0)
-            started.append(self.chip())
+            if self.single:
+                part(self.kept, 0)
+            else:
+                lax.fori_loop(0, 2, part, 0)
+
+        def when_kept(self, body):
+            if self.single:
+                pl.when(self.keep)(body)
+            else:
+                body()
 
         def chip_sum(self):
             mark("cs%d" % self.n)
+            self.when_kept(self.chip_sum_kept)
+
+        def chip_sum_kept(self):
             self.chip().wait_recv()
 
             def add(i, carry):
@@ -646,6 +727,9 @@
 
         def join(self):
             mark("jn%d" % self.n)
+            self.when_kept(self.join_kept)
+
+        def join_kept(self):
             @pl.when(self.odd)
             def _():
                 remote(
@@ -664,6 +748,13 @@
                 self.out_near(self.k).start()
 
         def drain(self):
+            if self.single:
+                pl.when(jnp.logical_not(self.keep))(lambda: self.chip().wait_send())
+            else:
+                self.chip().wait_send()
+            self.when_kept(self.drain_kept)
+
+        def drain_kept(self):
             @pl.when(self.far)
             def _():
                 self.out_far(0).wait_send()
@@ -674,38 +765,48 @@
                 self.out_near(1 - self.k).wait_send()
                 self.out_near(self.k).wait_send()
 
-    steps = [Step(n) for n in range(8)]
+    steps = [Step(n) for n in range(9)]
     steps[0].compute()
     mark("lev2_1")
-    level2(1)
-    level4(1, (0,))
-    steps[1].compute()
+    level2b(1, 0)
+    level2a(1, 0)
+    level2b(1, 1)
+    steps[2].compute()
     steps[0].chip_sum()
-    steps[2].compute()
-    steps[1].chip_sum()
     steps[3].compute()
     steps[2].chip_sum()
+    mark("w7")
+    level4(1, 0, (0,))
+    level4(1, 1, (0,))
+    steps[7].compute()
+    steps[3].chip_sum()
+    steps[1].compute()
+    steps[7].chip_sum()
+    steps[1].chip_sum()
+    mark("w4")
+    level4(1, 0, (1, 2))
+    level3(1, 1)
+    steps[4].compute()
     steps[0].join()
-    mark("lev3_1")
-    level3(1)
-    level4(1, (1, 2))
-    steps[4].compute()
-    steps[3].chip_sum()
-    steps[1].join()
+    steps[4].chip_sum()
+    mark("w30")
+    level3(1, 0)
+    steps[2].join()
+    steps[3].join()
+    mark("w5")
+    level4(1, 1, (1, 2))
     steps[5].compute()
-    steps[4].chip_sum()
-    steps[2].join()
+    steps[7].join()
     steps[6].compute()
     steps[5].chip_sum()
-    steps[3].join()
-    mark("lev4_1")
-    level4(1, (3,))
-    steps[7].compute()
+    steps[1].join()
+    mark("w8")
+    level4(1, 0, (3,))
+    level4(1, 1, (3,))
+    steps[8].compute()
     steps[6].chip_sum()
-    mark("d8")
-    steps[7].chip_sum()
-    for n in range(4, 8):
-        mark("j%d" % n)
+    steps[8].chip_sum()
+    for n in (4, 5, 6, 8):
         steps[n].join()
     mark("ewait")
 
@@ -760,9 +861,10 @@
         vmem((TOK, 2 * OC), BF16), vmem((TOK, HD), F32), vmem((TOK, FFL), F32), vmem((TOK, FFL), BF16),
         vmem((2, 8, TOK, SHARD), BF16), vmem((8, TOK, SHARD), BF16),
         vmem((8, TOK // 2, SHARD), BF16), vmem((2, 2, TOK, SHARD), BF16),
-        dma((13,)), dma((2, 2, 20)), dma((2, 2, 20)), dma((7,)), dma((7,)), dma((6,)), dma((6,)),
-        dma((9,)), dma((9,)), dma((9,)), dma((9,)), dma((8,)), dma((8,)), dma((8, 2)), dma((8,)),
-        dma((8, 2)), dma((2, 2, 2)),
+        vmem((2, 2, 128, OC), BF16),
+        dma((13,)), dma((2, 2, 20)), dma((2, 2, 20)), dma((13,)), dma((13,)), dma((6,)), dma((6,)),
+        dma((11,)), dma((11,)), dma((11,)), dma((11,)), dma((9,)), dma((9,)), dma((9, 2)), dma((9,)),
+        dma((9, 2)), dma((2, 2, 2)),
     ]
     return pl.pallas_call(
         kernel,

time: 141 us -> 125 us (0.89)
  Pallas kernels: 137 us -> 123 us
    pallas_call x1, Pallas kernels: 137 us -> 123 us  [per_device(): pl.pallas_call(kernel, out_shape=jax.ShapeDtypeStruct((TOK, OC), BF16), i...]
where the time goes in v3:
time: 125 us
  Pallas kernels  123 us (98%)
  local copies, waits for them, and re-layouts  2.06 us (2%)
    pallas_call x1, Pallas kernels, per_device(): pl.pallas_call(kernel, out_shape=jax.ShapeDtypeStruct((TOK, OC), BF16), i...  123 us

profile of v3, /device:TPU:17, one launch (start us, length us, event | category | flops | bytes accessed | tf_op | source)
XLA Modules:
  0.0 124.7 jit_solution(6690662163220757258)
XLA Ops:
  0.0 122.6 %layer.1 = bf16[768,512]{1,0:T(8,128)(2,1)} custom-call(bf16[768,512]{1,0:T(8,128)(2,1)} %residual.1, bf16[768,256]{1,0:T(8,128)(2,1)} %values.1, bf16[768,256]{1,0:T(8,128)(2,1)} %f_on.1, bf16[768,256]{1,0:T(8,128)(2,1)} %f_rev.1, f32[2,768]{1,0:T(2,128)} %bitcast.4, f32[2,256]{1,0:T(2,128)} %glc.1, bf16[768,256]{1,0:T(8,128)(2,1)} %query.1, ...), custom_call_target="tpu_custom_call" | custom-call | tf_op jit(solution)/shard_map/layer/pallas_call | solution.py:869
  122.6 2.1 %copy.15 = bf16[768,512]{1,0:T(8,128)(2,1)} copy(bf16[768,512]{1,0:T(8,128)(2,1)} %layer.1) | data formatting | bytes 1572864

commit v4 on v3

--- a/solution.py
+++ b/solution.py
@@ -46,7 +46,7 @@
     wu, wd, owc, ga, xa,
     qd, kr, sx, em, elx, run_state, run_log, row_in, col_in, sin, o_v, att,
     xg, ss, acc, hid,
-    pp, d2r, ra, ee, relay,
+    pp, d2r, ra, ee, relay, rel,
     in_sem, w_send, w_recv, ow_send, ow_recv, st_send, st_recv,
     g_send, g_recv, x_send, x_recv, c_send, c_recv, r_send, r_recv, e_send, e_recv,
 ):
@@ -278,10 +278,9 @@
         )
         run = dot(sums[d], split3(jnp.log1p(-key) + sg))
         mid, end = run[mid_at : mid_at + 1, :], run[end_at : end_at + 1, :]
-        q = que_v[rows, :].astype(F32)
-        q = q * sigmoid(q) * (HD ** -0.5)
-        qd[d, rows, :] = (q * jnp.exp(run - mid)).astype(BF16)
-        k = key * jnp.exp(mid - run)
+        away = mid - run
+        rel[d, rows, :] = away
+        k = key * jnp.exp(away)
         kr[d, rows, :] = k.astype(BF16)
         tail = (k * jnp.exp(end - mid)).astype(BF16)
         v = val_v[rows, :]
@@ -359,6 +358,10 @@
     def pass2_block(blk):
         rows = pl.ds(pl.multiple_of(blk * BLK, BLK), BLK)
         v = val_v[rows, :]
+        q = que_v[rows, :].astype(F32)
+        q = q * sigmoid(q) * (HD ** -0.5)
+        for d in range(2):
+            qd[d, rows, :] = (q * jnp.exp(-rel[d, rows, :])).astype(BF16)
         for h in range(HEADS):
             hs = slice(h * HD, (h + 1) * HD)
             fwd = dot(qd[0, rows, hs], kr[0, rows, hs], LAST)
@@ -478,22 +481,31 @@
             left, right = 2 * ym + core, 2 * yp + core
             self.got(0, left, 0)
             self.go(4, left, 0, right)
+            self.go(7, left, 0, partner)
             self.got(3, right, 1)
             self.go(5, right, 1, left)
+            self.go(8, right, 1, partner)
 
         def from_side(self):
             left, right = 2 * ym + core, 2 * yp + core
             self.got(1, left, 1)
-            self.go(7, left, None, partner)
+            self.go(9, left, 1, partner)
             self.got(2, right, 0)
-            self.go(8, right, None, partner)
+            self.go(10, right, 0, partner)
 
         def from_far(self):
             far = 2 * y2 + core
             self.got(4, far, 0)
-            self.go(9, far, 0, partner)
+            self.go(11, far, 0, partner)
             self.got(5, far, 1)
-            self.go(10, far, 1, partner)
+            self.go(12, far, 1, partner)
+
+        def other_core(self, chip):
+            block = 2 * chip + other
+            for k, part in {id(ym): ((7, 0), (9, 1)), id(yp): ((8, 1), (10, 0)), id(y2): ((11, 0), (12, 1))}[
+                id(chip)
+            ]:
+                self.got(k, block, part)
 
     gathered = Gather(ga, g_send, g_recv)
     mark("gown")
@@ -534,15 +546,14 @@
     level2b(0, 1)
     level0a(1)
     mark("gpart2")
-    gathered.got(7, 2 * ym + other, None)
+    gathered.other_core(ym)
     project(2 * ym + other)
-    gathered.got(8, 2 * yp + other, None)
+    gathered.other_core(yp)
     project(2 * yp + other)
     mark("gfar")
     gathered.from_far()
     project(2 * y2 + core)
-    gathered.got(9, 2 * y2 + other, 0)
-    gathered.got(10, 2 * y2 + other, 1)
+    gathered.other_core(y2)
     project(2 * y2 + other)
 
     TILE = 128
@@ -578,6 +589,16 @@
             cols = pl.ds(pl.multiple_of(n * 256, 256), 256)
             part = dot(xg[...], wu[pl.ds(pl.multiple_of(chip * 2 * OC, 2 * OC), 2 * OC), cols])
             acc[:, cols] = part if first else acc[:, cols] + part
+            return carry
+
+        lax.fori_loop(0, FFL // 256, tile, 0)
+
+    def lift_one(chip, c):
+        def tile(n, carry):
+            cols = pl.ds(pl.multiple_of(n * 256, 256), 256)
+            rows = pl.ds(pl.multiple_of((chip * 2 + c) * OC, OC), OC)
+            part = dot(xg[:, pl.ds(pl.multiple_of(c * OC, OC), OC)], wu[rows, cols])
+            acc[:, cols] = acc[:, cols] + part
             return carry
 
         lax.fori_loop(0, FFL // 256, tile, 0)
@@ -595,34 +616,36 @@
     spread.forward()
     mark("lev1a_1")
     level1a(1)
-    mark("xside")
-    spread.from_side()
     mark("lev4_0")
     level4(0, 0, range(4))
     level4(0, 1, range(4))
     mark("lift0")
     lift(y, True)
+    mark("xside")
+    spread.from_side()
     mark("lift1")
     scale(ym, core)
-    spread.got(7, 2 * ym + other, None)
+    lift_one(ym, core)
+    spread.other_core(ym)
     scale(ym, other)
-    lift(ym)
+    lift_one(ym, other)
     mark("lev1_1")
     level1b(1)
-    level2a(1, 1)
     mark("lift2")
     scale(yp, core)
-    spread.got(8, 2 * yp + other, None)
+    spread.other_core(yp)
     scale(yp, other)
     lift(yp)
+    mark("lev2a_1")
+    level2a(1, 1)
     mark("xfar")
     spread.from_far()
     mark("lift3")
     scale(y2, core)
-    spread.got(9, 2 * y2 + other, 0)
-    spread.got(10, 2 * y2 + other, 1)
+    lift_one(y2, core)
+    spread.other_core(y2)
     scale(y2, other)
-    lift(y2)
+    lift_one(y2, other)
 
     def activate(i, carry):
         rows = pl.ds(pl.multiple_of(i * TILE, TILE), TILE)
@@ -767,12 +790,12 @@
 
     steps = [Step(n) for n in range(9)]
     steps[0].compute()
+    steps[0].chip_sum()
     mark("lev2_1")
     level2b(1, 0)
     level2a(1, 0)
     level2b(1, 1)
     steps[2].compute()
-    steps[0].chip_sum()
     steps[3].compute()
     steps[2].chip_sum()
     mark("w7")
@@ -799,14 +822,15 @@
     steps[7].join()
     steps[6].compute()
     steps[5].chip_sum()
-    steps[1].join()
     mark("w8")
     level4(1, 0, (3,))
     level4(1, 1, (3,))
     steps[8].compute()
     steps[6].chip_sum()
+    steps[1].join()
+    steps[4].join()
     steps[8].chip_sum()
-    for n in (4, 5, 6, 8):
+    for n in (5, 6, 8):
         steps[n].join()
     mark("ewait")
 
@@ -825,18 +849,15 @@
             rows = pl.ds(pl.multiple_of(i * TILE, TILE), TILE)
             total = pp[1, slot, rows, :].astype(F32)
             total = total + (ee[0, dx, rows, :].astype(F32) + ee[1, dx, rows, :].astype(F32))
-            res_v[rows, cols] = (xa[tp, rows, cols].astype(F32) + total).astype(BF16)
+            out[rows, cols] = (xa[tp, rows, cols].astype(F32) + total).astype(BF16)
             return carry
 
         lax.fori_loop(0, TOK // TILE, finish, 0)
     mark("final")
-    final = pltpu.make_async_copy(res_v, out, in_sem.at[0])
-    final.start()
     for copy in started:
         copy.wait_send()
     for step in steps:
         step.drain()
-    final.wait()
     mark(None)
 
 
@@ -861,16 +882,16 @@
         vmem((TOK, 2 * OC), BF16), vmem((TOK, HD), F32), vmem((TOK, FFL), F32), vmem((TOK, FFL), BF16),
         vmem((2, 8, TOK, SHARD), BF16), vmem((8, TOK, SHARD), BF16),
         vmem((8, TOK // 2, SHARD), BF16), vmem((2, 2, TOK, SHARD), BF16),
-        vmem((2, 2, 128, OC), BF16),
+        vmem((2, 2, 128, OC), BF16), vmem((2, TOK, CH), F32),
         dma((13,)), dma((2, 2, 20)), dma((2, 2, 20)), dma((13,)), dma((13,)), dma((6,)), dma((6,)),
-        dma((11,)), dma((11,)), dma((11,)), dma((11,)), dma((9,)), dma((9,)), dma((9, 2)), dma((9,)),
+        dma((13,)), dma((13,)), dma((13,)), dma((13,)), dma((9,)), dma((9,)), dma((9, 2)), dma((9,)),
         dma((9, 2)), dma((2, 2, 2)),
     ]
     return pl.pallas_call(
         kernel,
-        out_shape=jax.ShapeDtypeStruct((TOK, OC), BF16),
+        out_shape=pltpu.VMEM((TOK, OC), BF16),
         in_specs=[any_spec] * 13,
-        out_specs=any_spec,
+        out_specs=pl.BlockSpec(memory_space=pltpu.VMEM),
         scratch_shapes=scratch,
         compiler_params=pltpu.CompilerParams(
             collective_id=0, has_side_effects=True, vmem_limit_bytes=66_000_000

time: 125 us -> 123 us (0.984)
  no operation moved by 1% of the time
where the time goes in v4:
time: 123 us
  Pallas kernels  122 us (99%)
    pallas_call x1, Pallas kernels, per_device(): pl.pallas_call(kernel, out_shape=pltpu.VMEM((TOK, OC), BF16), in_specs=[a...  122 us

profile of v4, /device:TPU:17, one launch (start us, length us, event | category | flops | bytes accessed | tf_op | source)
XLA Modules:
  0.0 122.9 jit_solution(17059223233357212133)
XLA Ops:
  0.0 122.0 %layer.1 = bf16[768,512]{1,0:T(8,128)(2,1)S(1)} custom-call(bf16[768,512]{1,0:T(8,128)(2,1)} %residual.1, bf16[768,256]{1,0:T(8,128)(2,1)} %values.1, bf16[768,256]{1,0:T(8,128)(2,1)} %f_on.1, bf16[768,256]{1,0:T(8,128)(2,1)} %f_rev.1, f32[2,768]{1,0:T(2,128)} %bitcast.4, f32[2,256]{1,0:T(2,128)} %glc.1, bf16[768,256]{1,0:T(8,128)(2,1)} %query.1, ...), custom_call_target="tpu_custom_call" | custom-call | tf_op jit(solution)/shard_map/layer/pallas_call | solution.py:890
  122.0 0.9 copy.15

commit v5 on v4

--- a/solution.py
+++ b/solution.py
@@ -73,10 +73,11 @@
     partner = 2 * y + other
 
     barrier = pltpu.get_barrier_semaphore()
-    for o in range(1, 16):
-        pl.semaphore_signal(barrier, inc=1, device_id=(lax.rem(sp + o, 16), tp), device_id_type=MESH)
-    for o in range(1, 8):
-        pl.semaphore_signal(barrier, inc=1, device_id=(sp, lax.rem(tp + o, 8)), device_id_type=MESH)
+    peers = [(z * 4 + ring(x, o), tp) for o in (1, 3, 2)]
+    peers += [(ring(z, o) * 4 + x, tp) for o in (1, 3, 2)]
+    peers += [(sp, 2 * near + c) for near in (yp, ym) for c in range(2)] + [(sp, partner)]
+    for peer in peers:
+        pl.semaphore_signal(barrier, inc=1, device_id=peer, device_id_type=MESH)
 
     own_rows = pl.ds(pl.multiple_of(sp * SHARD, SHARD), SHARD)
     ow_rows = pl.ds(pl.multiple_of(tp * 256, 256), 256)
@@ -91,7 +92,7 @@
     for copy in loads:
         copy.start()
 
-    pl.semaphore_wait(barrier, 22)
+    pl.semaphore_wait(barrier, len(peers))
 
     def remote(src, dst, ss_, rs_, dev):
         return pltpu.make_async_remote_copy(
@@ -659,14 +660,15 @@
 
 
     SHARDS = (
-        (1, 0), (0, 0), (1, 1), (1, -1), (1, 2), (0, 1), (0, -1), (0, 2), (2, 2)
+        (1, 0), (0, 0), (1, 1), (1, -1), (1, 2),
+        (0, 1), (0, -1), (0, 2), (2, 2), (2, 1), (2, -1),
     )
 
     class Step:
         def __init__(self, n):
             self.n = n
             dx, dz = SHARDS[n]
-            self.single = n >= 7
+            self.single = n >= 5
             self.dx = dx % 2
             zs = ring(z, dz)
             column = lax.rem(x + dx, 2)
@@ -700,21 +702,29 @@
                 e_send.at[self.n, k], e_recv.at[self.k, self.dx, k], (sp, self.to),
             )
 
-        def compute(self):
+        def compute(self, *others):
             mark("comp%d" % self.n)
-            def part(i, carry):
-                first = (self.first + 2 * (other + i * (core - other))) * SHARD
+
+            def part(j, carry):
+                i, first, slot = j, self.first, self.slot
+                if others:
+                    i = self.kept
+                    first = first + j * (others[0].first - first)
+                    slot = slot + j * (others[0].slot - slot)
+                elif self.single:
+                    i = self.kept
+                first = (first + 2 * (other + i * (core - other))) * SHARD
                 rows = wd[pl.ds(pl.multiple_of(first, SHARD), SHARD), :]
-                pp[i, self.slot] = dot(hid[...], rows, LAST).astype(BF16)
-
-                @pl.when(i == 0)
-                def _():
-                    self.chip().start()
-
+                pp[i, slot] = dot(hid[...], rows, LAST).astype(BF16)
+                if others:
+                    for g, step in enumerate((self, *others)):
+                        pl.when(jnp.logical_and(i == 0, j == g))(lambda step=step: step.chip().start())
+                else:
+                    pl.when(i == 0)(lambda: self.chip().start())
                 return carry
 
-            if self.single:
-                part(self.kept, 0)
+            if self.single and not others:
+                part(0, 0)
             else:
                 lax.fori_loop(0, 2, part, 0)
 
@@ -788,14 +798,17 @@
                 self.out_near(1 - self.k).wait_send()
                 self.out_near(self.k).wait_send()
 
-    steps = [Step(n) for n in range(9)]
+    steps = [Step(n) for n in range(11)]
     steps[0].compute()
+    steps[5].compute(steps[6])
     steps[0].chip_sum()
+    steps[5].chip_sum()
     mark("lev2_1")
     level2b(1, 0)
     level2a(1, 0)
     level2b(1, 1)
     steps[2].compute()
+    steps[6].chip_sum()
     steps[3].compute()
     steps[2].chip_sum()
     mark("w7")
@@ -815,22 +828,23 @@
     mark("w30")
     level3(1, 0)
     steps[2].join()
+    steps[5].join()
+    steps[6].join()
     steps[3].join()
     mark("w5")
     level4(1, 1, (1, 2))
-    steps[5].compute()
+    steps[9].compute(steps[10])
     steps[7].join()
-    steps[6].compute()
-    steps[5].chip_sum()
+    steps[9].chip_sum()
+    steps[10].chip_sum()
+    steps[4].join()
     mark("w8")
     level4(1, 0, (3,))
     level4(1, 1, (3,))
     steps[8].compute()
-    steps[6].chip_sum()
+    steps[8].chip_sum()
     steps[1].join()
-    steps[4].join()
-    steps[8].chip_sum()
-    for n in (5, 6, 8):
+    for n in (9, 10, 8):
         steps[n].join()
     mark("ewait")
 
@@ -884,8 +898,8 @@
         vmem((8, TOK // 2, SHARD), BF16), vmem((2, 2, TOK, SHARD), BF16),
         vmem((2, 2, 128, OC), BF16), vmem((2, TOK, CH), F32),
         dma((13,)), dma((2, 2, 20)), dma((2, 2, 20)), dma((13,)), dma((13,)), dma((6,)), dma((6,)),
-        dma((13,)), dma((13,)), dma((13,)), dma((13,)), dma((9,)), dma((9,)), dma((9, 2)), dma((9,)),
-        dma((9, 2)), dma((2, 2, 2)),
+        dma((13,)), dma((13,)), dma((13,)), dma((13,)), dma((11,)), dma((11,)), dma((11, 2)), dma((11,)),
+        dma((11, 2)), dma((2, 2, 2)),
     ]
     return pl.pallas_call(
         kernel,

time: 123 us -> 121 us (0.984)
  Pallas kernels: 122 us -> 120 us
    pallas_call x1, Pallas kernels: 122 us -> 120 us  [per_device(): pl.pallas_call(kernel, out_shape=pltpu.VMEM((TOK, OC), BF16), in_specs=[a...]
where the time goes in v5:
time: 121 us; the launch traced here: 120 us
  Pallas kernels  120 us (99%)
    pallas_call x1, Pallas kernels, per_device(): pl.pallas_call(kernel, out_shape=pltpu.VMEM((TOK, OC), BF16), in_specs=[a...  120 us

profile of v5, /device:TPU:17, one launch (start us, length us, event | category | flops | bytes accessed | tf_op | source)
XLA Modules:
  0.0 120.4 jit_solution(10586075905939126143)
XLA Ops:
  0.0 119.5 %layer.1 = bf16[768,512]{1,0:T(8,128)(2,1)S(1)} custom-call(bf16[768,512]{1,0:T(8,128)(2,1)} %residual.1, bf16[768,256]{1,0:T(8,128)(2,1)} %values.1, bf16[768,256]{1,0:T(8,128)(2,1)} %f_on.1, bf16[768,256]{1,0:T(8,128)(2,1)} %f_rev.1, f32[2,768]{1,0:T(2,128)} %bitcast.4, f32[2,256]{1,0:T(2,128)} %glc.1, bf16[768,256]{1,0:T(8,128)(2,1)} %query.1, ...), custom_call_target="tpu_custom_call" | custom-call | tf_op jit(solution)/shard_map/layer/pallas_call | solution.py:904
  119.5 0.9 copy.15

commit v6 on v5

--- a/solution.py
+++ b/solution.py
@@ -154,12 +154,14 @@
         src = weights[t][0].at[pl.ds(half * 2 * QUARTER, 2 * QUARTER)]
         w_second(t, half, 0, src=src)
 
-    def level1a(t):
+    def level1p(t):
         for half in range(2):
             w_got(t, half, 0, -1, 0, None)
             w_go(t, half, 2, -1, 0, 0, (1, 0))
             w_got(t, half, 1, 1, 0, None)
             w_go(t, half, 3, 1, 0, 1, (-1, 0))
+
+    def level1s(t):
         for half in range(2):
             w_second(t, half, 1)
             w_second(t, half, 2)
@@ -355,6 +357,7 @@
         started.append(copy)
     mark("l0b")
     level0b(0, 0)
+    level0b(0, 1)
 
     def pass2_block(blk):
         rows = pl.ds(pl.multiple_of(blk * BLK, BLK), BLK)
@@ -384,6 +387,7 @@
 
     mark("owfwd")
     ow_forward()
+    level1p(0)
     mark("roww")
     for o in (1, 3, 2):
         row_got(o)
@@ -407,12 +411,11 @@
         copy = col_copy(o)
         copy.start()
         started.append(copy)
-    level0b(0, 1)
     sin[...] = jnp.zeros_like(sin)
     mark("colw")
     for o in (1, 3, 2):
         col_got(o)
-    level1a(0)
+    level1s(0)
     mark("combine")
 
     def chain(ref, at):
@@ -616,7 +619,8 @@
     mark("xfwd")
     spread.forward()
     mark("lev1a_1")
-    level1a(1)
+    level1p(1)
+    level1s(1)
     mark("lev4_0")
     level4(0, 0, range(4))
     level4(0, 1, range(4))
@@ -810,20 +814,21 @@
     steps[2].compute()
     steps[6].chip_sum()
     steps[3].compute()
-    steps[2].chip_sum()
     mark("w7")
     level4(1, 0, (0,))
     level4(1, 1, (0,))
     steps[7].compute()
+    steps[2].chip_sum()
     steps[3].chip_sum()
+    steps[7].chip_sum()
     steps[1].compute()
-    steps[7].chip_sum()
     steps[1].chip_sum()
     mark("w4")
     level4(1, 0, (1, 2))
     level3(1, 1)
     steps[4].compute()
     steps[0].join()
+    steps[7].join()
     steps[4].chip_sum()
     mark("w30")
     level3(1, 0)
@@ -834,7 +839,6 @@
     mark("w5")
     level4(1, 1, (1, 2))
     steps[9].compute(steps[10])
-    steps[7].join()
     steps[9].chip_sum()
     steps[10].chip_sum()
     steps[4].join()

time: 121 us -> 118 us (0.975)
  Pallas kernels: 120 us -> 117 us
    pallas_call x1, Pallas kernels: 120 us -> 117 us  [per_device(): pl.pallas_call(kernel, out_shape=pltpu.VMEM((TOK, OC), BF16), in_specs=[a...]
where the time goes in v6:
time: 118 us
  Pallas kernels  117 us (99%)
    pallas_call x1, Pallas kernels, per_device(): pl.pallas_call(kernel, out_shape=pltpu.VMEM((TOK, OC), BF16), in_specs=[a...  117 us

profile of v6, /device:TPU:17, one launch (start us, length us, event | category | flops | bytes accessed | tf_op | source)
XLA Modules:
  0.0 118.1 jit_solution(11482193239290493183)
XLA Ops:
  0.0 117.2 %layer.1 = bf16[768,512]{1,0:T(8,128)(2,1)S(1)} custom-call(bf16[768,512]{1,0:T(8,128)(2,1)} %residual.1, bf16[768,256]{1,0:T(8,128)(2,1)} %values.1, bf16[768,256]{1,0:T(8,128)(2,1)} %f_on.1, bf16[768,256]{1,0:T(8,128)(2,1)} %f_rev.1, f32[2,768]{1,0:T(2,128)} %bitcast.4, f32[2,256]{1,0:T(2,128)} %glc.1, bf16[768,256]{1,0:T(8,128)(2,1)} %query.1, ...), custom_call_target="tpu_custom_call" | custom-call | tf_op jit(solution)/shard_map/layer/pallas_call | solution.py:908
  117.2 0.9 copy.15

commit v7 on v6

--- a/solution.py
+++ b/solution.py
@@ -412,10 +412,10 @@
         copy.start()
         started.append(copy)
     sin[...] = jnp.zeros_like(sin)
+    level1s(0)
     mark("colw")
     for o in (1, 3, 2):
         col_got(o)
-    level1s(0)
     mark("combine")
 
     def chain(ref, at):

time: 118 us -> 117 us (level)
  no operation moved by 1% of the time
where the time goes in v7:
time: 117 us
  Pallas kernels  116 us (99%)
    pallas_call x1, Pallas kernels, per_device(): pl.pallas_call(kernel, out_shape=pltpu.VMEM((TOK, OC), BF16), in_specs=[a...  116 us

profile of v7, /device:TPU:17, one launch (start us, length us, event | category | flops | bytes accessed | tf_op | source)
XLA Modules:
  0.0 117.4 jit_solution(10334939834418510426)
XLA Ops:
  0.0 116.5 %layer.1 = bf16[768,512]{1,0:T(8,128)(2,1)S(1)} custom-call(bf16[768,512]{1,0:T(8,128)(2,1)} %residual.1, bf16[768,256]{1,0:T(8,128)(2,1)} %values.1, bf16[768,256]{1,0:T(8,128)(2,1)} %f_on.1, bf16[768,256]{1,0:T(8,128)(2,1)} %f_rev.1, f32[2,768]{1,0:T(2,128)} %bitcast.4, f32[2,256]{1,0:T(2,128)} %glc.1, bf16[768,256]{1,0:T(8,128)(2,1)} %query.1, ...), custom_call_target="tpu_custom_call" | custom-call | tf_op jit(solution)/shard_map/layer/pallas_call | solution.py:908
  116.5 0.9 copy.15
